TPU v7x, 256 devices: a whole 4x4x8 slice. The times are simulated.
256 devices in a mesh: st: 64 (over z, y, core), tp: 4 (over x).
Axes of the slice: x: 4, y: 4, z: 8, core: 2. Of those that a mesh axis runs over, the one named last changes fastest.
Arguments:
- tokens: bfloat16 [24576, 2048], P('st', 'tp'), may hold values from -6 to 6
- cotangent: bfloat16 [24576, 1024], P('st', 'tp'), may hold values from -48 to 48
- mix_query: bfloat16 [24576, 1024], P('st', 'tp'), may hold values from -6 to 6
- mix_key: bfloat16 [24576, 1024], P('st', 'tp'), may hold values from -6 to 6
- mix_value: bfloat16 [24576, 1024], P('st', 'tp'), may hold values from -24 to 24
- beta_pre: float32 [8, 24576], P('tp', 'st'), may hold values from -9 to 9
- decay_pre: float32 [8, 24576], P('tp', 'st'), may hold values from -8 to 6
- decay_rate: float32 [8], P('tp'), may hold values from 0.001 to 0.06
- passages: bfloat16 [1024, 64, 2048], P('st'), may hold values from -16 to 16
- passage_ids: int32 [384, 4], P('st'), may hold values from 0 to 1023, as said below
- query_weight: bfloat16 [2048, 1024], P(None, 'tp'), may hold values from -0.125 to 0.125
- key_weight: bfloat16 [2048, 1024], P(None, 'tp'), may hold values from -0.125 to 0.125
- value_weight: bfloat16 [2048, 1024], P(None, 'tp'), may hold values from -0.125 to 0.125
- gate_weight: bfloat16 [4, 2048], P('tp'), may hold values from -0.125 to 0.125
Outputs:
- token_grad: bfloat16 [24576, 2048], P('st', 'tp')
- passage_grad: bfloat16 [1024, 64, 2048], P('st', None, 'tp')
- key_weight_grad: float32 [2048, 1024], P('st', 'tp')
Inputs may be any that keep to these rules, and one draw needn't show every extreme that they name: Passage p is stored on index p // 16 of st. The rows of passage_ids read by one index of st name at most 1 passages stored on any one index of st, and exactly 1 on some.
All inputs are finite; a program needn't handle non-finite values.
Results may differ from a plain program's by a relative error of at most 0.012.
The roundings to bfloat16 on the way count: a program that leaves them out, or rounds other values in their place, can miss the bound.
Values may be sent and summed in bfloat16 or wider, within the bound.
A program may use at most 128 MiB of HBM per device.

v0:
```python
import functools

import jax
import jax.numpy as jnp
from jax import lax
from jax.experimental import pallas as pl
from jax.experimental.pallas import tpu as pltpu
from jax.sharding import PartitionSpec as P

SPAN = 64


NORM_FLOOR = 1.0
SCORE_GAIN = 4.0
HIGHEST = lax.Precision.HIGHEST
CONTRACT_LAST = (((1,), (1,)), ((), ()))
CONTRACT_FIRST = (((0,), (0,)), ((), ()))

MESH = pl.DeviceIdType.MESH
VMEM_SPEC = pl.BlockSpec(memory_space=pltpu.VMEM)
DMA = pltpu.SemaphoreType.DMA
CHUNK = 256


def tp_places():
    place = lax.axis_index("tp")
    parity = lax.rem(place, 2)
    half = place // 2
    return place, parity, half, place + 1 - 2 * parity, lax.rem(place + 2, 4)


def st_peer(me, step, st_count):
    half = st_count // 2
    side, place = me // half, lax.rem(me, half)
    if step <= half:
        return (1 - side) * half + lax.rem(place + step - 1, half)
    return side * half + lax.rem(place + step - half, half)


def meet(st_count, with_st, with_tp=True):
    barrier = pltpu.get_barrier_semaphore()
    _, _, _, partner, far = tp_places()
    for other in (partner, far) if with_tp else ():
        pl.semaphore_signal(barrier, inc=1, device_id={"tp": other}, device_id_type=MESH)
    total = 2 if with_tp else 0
    if with_st:
        me = lax.axis_index("st")
        for step in range(1, st_count):
            pl.semaphore_signal(
                barrier,
                inc=1,
                device_id={"st": st_peer(me, step, st_count)},
                device_id_type=MESH,
            )
        total += st_count - 1
    pl.semaphore_wait(barrier, total)


def scatter_sum(term, out_ref, chunks, first_send, first_recv, kept, second_send, second_recv, sems):
    _, parity, half, partner, far = tp_places()
    send_a, recv_a, send_b, recv_b = sems
    rows = out_ref.shape[0] // chunks

    def pair_copy(k, i):
        return pltpu.make_async_remote_copy(
            src_ref=first_send.at[k, i],
            dst_ref=first_recv.at[k, i],
            send_sem=send_a.at[k, i],
            recv_sem=recv_a.at[k, i],
            device_id={"tp": partner},
            device_id_type=MESH,
        )

    def far_copy(k):
        return pltpu.make_async_remote_copy(
            src_ref=second_send.at[k],
            dst_ref=second_recv.at[k],
            send_sem=send_b.at[k],
            recv_sem=recv_b.at[k],
            device_id={"tp": far},
            device_id_type=MESH,
        )

    def pass_on(k):
        pair_copy(k, 0).wait_recv()
        second_send[k] = (
            kept[k, 0].astype(jnp.float32) + first_recv[k, 0].astype(jnp.float32)
        ).astype(jnp.bfloat16)
        far_copy(k).start()

    for k in range(chunks):
        for i in range(2):
            column = 2 * (1 - half if i == 0 else half)
            first_send[k, i] = term(k, column + 1 - parity).astype(jnp.bfloat16)
            pair_copy(k, i).start()
            kept[k, i] = term(k, column + parity).astype(jnp.bfloat16)
            if i == 0 and k >= 1:
                pass_on(k - 1)
    pass_on(chunks - 1)
    for k in range(chunks):
        pair_copy(k, 1).wait_recv()
        far_copy(k).wait_recv()
        out_ref[pl.ds(k * rows, rows), :] = (
            kept[k, 1].astype(jnp.float32)
            + first_recv[k, 1].astype(jnp.float32)
            + second_recv[k].astype(jnp.float32)
        ).astype(out_ref.dtype)
    for k in range(chunks):
        pair_copy(k, 0).wait_send()
        pair_copy(k, 1).wait_send()
        far_copy(k).wait_send()


def scatter_scratch(chunks, rows, width):
    return [
        pltpu.VMEM((chunks, 2, rows, width), jnp.bfloat16),
        pltpu.VMEM((chunks, 2, rows, width), jnp.bfloat16),
        pltpu.VMEM((chunks, 2, rows, width), jnp.bfloat16),
        pltpu.VMEM((chunks, rows, width), jnp.bfloat16),
        pltpu.VMEM((chunks, rows, width), jnp.bfloat16),
        DMA((chunks, 2)),
        DMA((chunks, 2)),
        DMA((chunks,)),
        DMA((chunks,)),
    ]


def project_kernel(
    st_count,
    ids_ref,
    rows_hbm,
    kw_ref,
    vw_ref,
    ids_all_ref,
    key_ref,
    packed_ref,
    rows_ref,
    rows_sem,
    id_send,
    id_recv,
):
    me = lax.axis_index("st")
    head_dim = kw_ref.shape[1]
    chunks = rows_ref.shape[0] // CHUNK

    def rows_copy(k):
        here = pl.ds(k * CHUNK, CHUNK)
        return pltpu.make_async_copy(rows_hbm.at[here, :], rows_ref.at[here, :], rows_sem.at[k])

    for k in range(chunks):
        rows_copy(k).start()
    meet(st_count, True, False)

    def id_copy(step):
        return pltpu.make_async_remote_copy(
            src_ref=ids_ref,
            dst_ref=ids_all_ref.at[me],
            send_sem=id_send.at[step],
            recv_sem=id_recv.at[step],
            device_id={"st": st_peer(me, step, st_count)},
            device_id_type=MESH,
        )

    for step in range(1, st_count):
        id_copy(step).start()
    ids_all_ref[pl.ds(me, 1)] = ids_ref[...][None]

    for k in range(chunks):
        rows_copy(k).wait()
        here = pl.ds(k * CHUNK, CHUNK)
        block = rows_ref[here, :]
        key_low = jnp.dot(block, kw_ref[...], preferred_element_type=jnp.float32).astype(
            jnp.bfloat16
        )
        key_ref[here, :] = key_low
        key_float = key_low.astype(jnp.float32)
        scale = lax.rsqrt(jnp.mean(key_float * key_float, axis=-1, keepdims=True) + NORM_FLOOR)
        packed_ref[here, pl.ds(0, head_dim)] = (key_float * scale).astype(jnp.bfloat16)
        packed_ref[here, pl.ds(head_dim, head_dim)] = jnp.dot(
            block, vw_ref[...], preferred_element_type=jnp.float32
        ).astype(jnp.bfloat16)

    for step in range(1, st_count):
        id_copy(step).wait()


def project_call(st_count, ids_padded, flat_rows, key_weight, value_weight):
    head_dim = key_weight.shape[1]
    total_rows = flat_rows.shape[0]
    return pl.pallas_call(
        functools.partial(project_kernel, st_count),
        out_shape=(
            jax.ShapeDtypeStruct((st_count, *ids_padded.shape), jnp.int32),
            jax.ShapeDtypeStruct((total_rows, head_dim), jnp.bfloat16),
            jax.ShapeDtypeStruct((total_rows, 2 * head_dim), jnp.bfloat16),
        ),
        in_specs=[VMEM_SPEC, pl.BlockSpec(memory_space=pl.ANY), VMEM_SPEC, VMEM_SPEC],
        out_specs=(VMEM_SPEC,) * 3,
        scratch_shapes=[
            pltpu.VMEM(flat_rows.shape, jnp.bfloat16),
            DMA((total_rows // CHUNK,)),
            DMA((st_count,)),
            DMA((st_count,)),
        ],
        compiler_params=pltpu.CompilerParams(collective_id=0, has_side_effects=True),
        name="ids_project",
    )(ids_padded, flat_rows, key_weight, value_weight)


def settle_kernel(*refs):
    count = len(refs) // 2
    for source, target in zip(refs[:count], refs[count:]):
        target[...] = source[...]


def settle_call(*arrays):
    return pl.pallas_call(
        settle_kernel,
        out_shape=tuple(jax.ShapeDtypeStruct(x.shape, x.dtype) for x in arrays),
        in_specs=[VMEM_SPEC] * len(arrays),
        out_specs=(VMEM_SPEC,) * len(arrays),
        name="settle",
    )(*arrays)


def exact_dot(left, right, dims=(((1,), (0,)), ((), ()))):
    return lax.dot_general(
        left, right, dims, precision=HIGHEST, preferred_element_type=jnp.float32
    )


def mixer_span(queries, keys_in, values_in, strength, log_decay, state):
    span = queries.shape[0]
    row_at = lax.broadcasted_iota(jnp.int32, (span, span), 0)
    col_at = lax.broadcasted_iota(jnp.int32, (span, span), 1)
    inclusive = row_at >= col_at
    unit_eye = jnp.where(row_at == col_at, 1.0, 0.0)
    decay_row = jnp.sum(unit_eye * log_decay, axis=0, keepdims=True)
    cum_row = jnp.sum(jnp.where(row_at <= col_at, log_decay, 0.0), axis=0, keepdims=True)
    cum_col = jnp.sum(jnp.where(inclusive, decay_row, 0.0), axis=1, keepdims=True)
    total = jnp.sum(log_decay, axis=0, keepdims=True)
    decay_map = jnp.exp(jnp.where(inclusive, cum_col - cum_row, -1e30))
    queries = (
        queries
        * lax.rsqrt(jnp.sum(queries * queries, axis=-1, keepdims=True) + NORM_FLOOR)
        * queries.shape[-1] ** (-0.5)
    )
    keys_in = keys_in * lax.rsqrt(jnp.sum(keys_in * keys_in, axis=-1, keepdims=True) + NORM_FLOOR)
    power = jnp.where(
        row_at > col_at, strength * exact_dot(keys_in, keys_in, CONTRACT_LAST) * decay_map, 0.0
    )
    inverse = unit_eye - power
    for _ in range(span.bit_length() - 2):
        power = exact_dot(power, power)
        inverse = exact_dot(inverse, unit_eye + power)
    attend = exact_dot(queries, keys_in, CONTRACT_LAST) * decay_map
    fresh = exact_dot(inverse, values_in * strength)
    correction = exact_dot(inverse, keys_in * (strength * jnp.exp(cum_col)))
    new_values = fresh - exact_dot(correction, state)
    output = exact_dot(queries * jnp.exp(cum_col), state) + exact_dot(attend, new_values)
    state = state * jnp.exp(total) + exact_dot(
        keys_in * jnp.exp(total - cum_col), new_values, CONTRACT_FIRST
    )
    return output, state


def main_kernel(
    st_count,
    sizes,
    local_ref,
    slot_ref,
    request_ref,
    rate_ref,
    code_ref,
    own_ref,
    packed_ref,
    key_ref,
    cot_ref,
    mq_ref,
    mk_ref,
    mv_ref,
    beta_ref,
    decay_ref,
    qw_ref,
    gate_ref,
    kw_ref,
    vw_ref,
    rows_hbm,
    tok_out,
    out_ref,
    weight_ref,
    tok_ref,
    tok_send,
    tok_recv,
    gw_ref,
    turned,
    rows_ref,
    rows_sem,
    send_buf,
    arrived,
    reply_rows,
    reply_send,
    reply_recv,
    x_sems,
    query_low,
    query_hat,
    query_grad,
    gate_grad,
    gate_open,
    mixed,
    states,
    block_kv,
    key_grad,
    value_grad,
    weight_send,
    weight_recv,
    w_send,
    w_recv,
    *scratch,
):
    cap, per_block, tok_chunks, row_chunks = sizes
    me = lax.axis_index("st")
    slot_total, span_rows, _ = send_buf.shape
    head_dim = key_ref.shape[1]
    part = weight_ref.shape[0]
    blocks_n = slot_ref.shape[0] // per_block
    block_rows = tok_ref.shape[0] // blocks_n
    heads_n = beta_ref.shape[0]
    mix_dim = mq_ref.shape[1] // heads_n
    score_scale = SCORE_GAIN * head_dim ** (-0.5)
    rows_copy = pltpu.make_async_copy(rows_hbm, rows_ref, rows_sem)
    rows_copy.start()
    meet(st_count, True)

    def exchange(lane, source, target, step):
        peer = st_peer(me, step, st_count)
        return pltpu.make_async_remote_copy(
            src_ref=source.at[pl.ds(peer * cap, cap)],
            dst_ref=target.at[pl.ds(me * cap, cap)],
            send_sem=x_sems.at[lane, 0, step],
            recv_sem=x_sems.at[lane, 1, step],
            device_id={"st": peer},
            device_id_type=MESH,
        )

    place, _, _, partner, far = tp_places()
    own_width = own_ref.shape[1]

    def tok_columns(which):
        return pl.ds(pl.multiple_of(which * own_width, own_width), own_width)

    def tok_copy(lane, source, which, target):
        return pltpu.make_async_remote_copy(
            src_ref=source,
            dst_ref=tok_ref.at[:, tok_columns(which)],
            send_sem=tok_send.at[lane],
            recv_sem=tok_recv.at[lane],
            device_id={"tp": target},
            device_id_type=MESH,
        )

    to_partner = tok_copy(0, own_ref, place, partner)
    to_far = tok_copy(1, own_ref, place, far)
    onward = tok_copy(2, tok_ref.at[:, tok_columns(far)], far, partner)
    to_far.start()
    for step in range(1, st_count):
        peer = st_peer(me, step, st_count)
        for c in range(cap):
            send_buf[peer * cap + c] = packed_ref[local_ref[peer * cap + c]]
        exchange(0, send_buf, arrived, step).start()
    for c in range(cap):
        arrived[me * cap + c] = packed_ref[local_ref[me * cap + c]]

    to_partner.start()
    tok_ref[:, tok_columns(place)] = own_ref[...]
    gw_ref[...] = gate_ref[...].astype(jnp.float32)
    turned[...] = jnp.transpose(
        jnp.concatenate(
            [
                beta_ref[...],
                decay_ref[...],
                jnp.zeros((8 - 2 * heads_n, beta_ref.shape[1]), jnp.float32),
            ],
            axis=0,
        )
    )
    states[...] = jnp.zeros_like(states)

    def mix(b):
        here = pl.ds(pl.multiple_of(b * SPAN, SPAN), SPAN)
        for m in range(heads_n):
            cols = pl.ds(m * mix_dim, mix_dim)
            raw = turned[here, heads_n + m : heads_n + m + 1]
            softplus = jnp.maximum(raw, 0.0) + jnp.log1p(jnp.exp(-jnp.abs(raw)))
            mixed[here, cols], states[m] = mixer_span(
                mq_ref[here, cols].astype(jnp.float32),
                mk_ref[here, cols].astype(jnp.float32),
                mv_ref[here, cols].astype(jnp.float32),
                jax.nn.sigmoid(turned[here, m : m + 1]),
                -rate_ref[m] * softplus,
                states[m],
            )

    spans_n = tok_ref.shape[0] // SPAN
    pl.loop(0, spans_n // 2)(mix)
    to_far.wait_recv()
    onward.start()
    pl.loop(spans_n // 2, spans_n)(mix)
    to_partner.wait_recv()
    onward.wait_recv()

    @pl.loop(0, blocks_n)
    def _(b):
        here = pl.ds(pl.multiple_of(b * block_rows, block_rows), block_rows)
        low = jnp.dot(tok_ref[here, :], qw_ref[...], preferred_element_type=jnp.float32).astype(
            jnp.bfloat16
        )
        query_low[here, :] = low
        low = low.astype(jnp.float32)
        scale = lax.rsqrt(jnp.mean(low * low, axis=-1, keepdims=True) + NORM_FLOOR)
        query_hat[here, :] = (low * scale).astype(jnp.bfloat16)
        gate_open[here, :] = jax.nn.sigmoid(
            jnp.sum(tok_ref[here, :].astype(jnp.float32) * gw_ref[...], axis=-1, keepdims=True)
        )

    for step in range(1, st_count):
        exchange(0, send_buf, arrived, step).wait_recv()

    @pl.loop(0, blocks_n)
    def _(b):
        here = pl.ds(pl.multiple_of(b * block_rows, block_rows), block_rows)
        for j in range(per_block):
            block_kv[pl.ds(j * span_rows, span_rows), :] = arrived[slot_ref[b * per_block + j]]
        keys = block_kv[:, :head_dim]
        values = block_kv[:, head_dim:]
        q_hat = query_hat[here, :]
        opened = gate_open[here, :]
        cot = cot_ref[here, :].astype(jnp.float32)
        grad_ret = (opened * cot).astype(jnp.bfloat16)
        exp_scores = jnp.exp(
            lax.dot_general(q_hat, keys, CONTRACT_LAST, preferred_element_type=jnp.float32)
            * score_scale
        )
        probs = exp_scores / jnp.sum(exp_scores, axis=-1, keepdims=True)
        probs_low = probs.astype(jnp.bfloat16)
        retrieved = jnp.dot(probs_low, values, preferred_element_type=jnp.float32)
        gate_grad[here, :] = (
            jnp.sum(cot * (retrieved - mixed[here, :]), axis=-1, keepdims=True)
            * opened
            * (1.0 - opened)
        )
        grad_probs = lax.dot_general(
            grad_ret, values, CONTRACT_LAST, preferred_element_type=jnp.float32
        )
        score_grad = (
            probs * (grad_probs - jnp.sum(grad_probs * probs, axis=-1, keepdims=True))
        ).astype(jnp.bfloat16)
        key_term = (
            score_scale
            * lax.dot_general(score_grad, q_hat, CONTRACT_FIRST, preferred_element_type=jnp.float32)
        ).astype(jnp.bfloat16)
        value_term = lax.dot_general(
            probs_low, grad_ret, CONTRACT_FIRST, preferred_element_type=jnp.float32
        ).astype(jnp.bfloat16)
        for j in range(per_block):
            piece = slice(j * span_rows, (j + 1) * span_rows)
            reply_rows[b * per_block + j, :, pl.ds(0, head_dim)] = key_term[piece]
            reply_rows[b * per_block + j, :, pl.ds(head_dim, head_dim)] = value_term[piece]
        hat_grad = score_scale * jnp.dot(score_grad, keys, preferred_element_type=jnp.float32)
        low = query_low[here, :].astype(jnp.float32)
        scale = lax.rsqrt(jnp.mean(low * low, axis=-1, keepdims=True) + NORM_FLOOR)
        query_grad[here, :] = (
            scale * hat_grad
            - scale * scale * scale * low * jnp.mean(low * hat_grad, axis=-1, keepdims=True)
        ).astype(jnp.bfloat16)

    for step in range(1, st_count):
        peer = st_peer(me, step, st_count)
        for c in range(cap):
            reply_send[peer * cap + c] = reply_rows[request_ref[peer * cap + c]]
        exchange(1, reply_send, reply_recv, step).start()
    for c in range(cap):
        reply_recv[me * cap + c] = reply_rows[request_ref[me * cap + c]]

    tok_width = tok_out.shape[1]
    tok_rows = tok_out.shape[0] // tok_chunks

    def token_term(k, which):
        here = pl.ds(k * tok_rows, tok_rows)
        cols = pl.ds(pl.multiple_of(which * tok_width, tok_width), tok_width)
        return (
            lax.dot_general(
                query_grad[here, :],
                qw_ref[cols, :],
                CONTRACT_LAST,
                preferred_element_type=jnp.float32,
            )
            + gate_grad[here, :] * gw_ref[:, cols]
        )

    scatter_sum(token_term, tok_out, tok_chunks, *scratch[:5], scratch[5:9])

    for step in range(1, st_count):
        exchange(1, reply_send, reply_recv, step).wait_recv()

    @pl.loop(0, out_ref.shape[0] // CHUNK)
    def _(k):
        here = pl.ds(pl.multiple_of(k * CHUNK, CHUNK), CHUNK)
        row_at = lax.broadcasted_iota(jnp.int32, (CHUNK, code_ref.shape[1]), 0) + k * CHUNK
        pick = jnp.where(row_at == code_ref[...], 1.0, 0.0).astype(jnp.bfloat16)
        summed = jnp.dot(
            pick,
            reply_recv[...].reshape(slot_total * span_rows, 2 * head_dim),
            preferred_element_type=jnp.float32,
        )
        hat_grad = summed[:, :head_dim]
        key_float = key_ref[here, :].astype(jnp.float32)
        scale = lax.rsqrt(jnp.mean(key_float * key_float, axis=-1, keepdims=True) + NORM_FLOOR)
        key_grad[here, :] = (
            scale * hat_grad
            - scale * scale * scale
            * key_float
            * jnp.mean(key_float * hat_grad, axis=-1, keepdims=True)
        ).astype(jnp.bfloat16)
        value_grad[here, :] = summed[:, head_dim:].astype(jnp.bfloat16)

    rows_copy.wait()

    def own_part(which):
        return weight_send.at[pl.ds(pl.multiple_of(which * part, part), part), :]

    def weight_copy(step):
        target = st_peer(me, step, st_count)
        return pltpu.make_async_remote_copy(
            src_ref=own_part(target),
            dst_ref=weight_recv.at[step],
            send_sem=w_send.at[step],
            recv_sem=w_recv.at[step],
            device_id={"st": target},
            device_id_type=MESH,
        )

    @pl.loop(0, weight_send.shape[0] // CHUNK)
    def _(k):
        here = pl.ds(pl.multiple_of(k * CHUNK, CHUNK), CHUNK)
        weight_send[here, :] = lax.dot_general(
            rows_ref[:, here], key_grad[...], CONTRACT_FIRST, preferred_element_type=jnp.float32
        ).astype(jnp.bfloat16)

    for step in range(1, st_count):
        weight_copy(step).start()

    width = out_ref.shape[1]
    rows = out_ref.shape[0] // row_chunks

    def row_term(k, which):
        here = pl.ds(k * rows, rows)
        cols = pl.ds(pl.multiple_of(which * width, width), width)
        return lax.dot_general(
            key_grad[here, :], kw_ref[cols, :], CONTRACT_LAST, preferred_element_type=jnp.float32
        ) + lax.dot_general(
            value_grad[here, :], vw_ref[cols, :], CONTRACT_LAST, preferred_element_type=jnp.float32
        )

    scatter_sum(row_term, out_ref, row_chunks, *scratch[9:14], scratch[14:18])
    weight_ref[...] = own_part(me)[...].astype(jnp.float32)
    for step in range(1, st_count):
        weight_copy(step).wait_recv()
        weight_ref[...] += weight_recv[step].astype(jnp.float32)
    for step in range(1, st_count):
        weight_copy(step).wait_send()
        exchange(0, send_buf, arrived, step).wait_send()
        exchange(1, reply_send, reply_recv, step).wait_send()
    to_partner.wait_send()
    to_far.wait_send()
    onward.wait_send()


def main_call(st_count, cap, per_block, span_rows, *operands):
    slot_local, tok, key_low, cot = operands[0], operands[5], operands[7], operands[8]
    flat_rows = operands[-1]
    heads_n = operands[12].shape[0]
    slot_total = slot_local.shape[0]
    tok_rows, model_width = tok.shape[0], flat_rows.shape[1]
    rows, head_dim = key_low.shape
    width = model_width // 4
    part = model_width // st_count
    tok_chunks, row_chunks = 3, 4
    mix_dim = cot.shape[1] // heads_n
    slots = pltpu.VMEM((slot_total, span_rows, 2 * head_dim), jnp.bfloat16)
    smem = pl.BlockSpec(memory_space=pltpu.SMEM)
    return pl.pallas_call(
        functools.partial(main_kernel, st_count, (cap, per_block, tok_chunks, row_chunks)),
        out_shape=(
            jax.ShapeDtypeStruct((tok_rows, width), jnp.bfloat16),
            jax.ShapeDtypeStruct((rows, width), jnp.bfloat16),
            jax.ShapeDtypeStruct((part, head_dim), jnp.float32),
        ),
        in_specs=[smem] * 4 + [VMEM_SPEC] * 14 + [pl.BlockSpec(memory_space=pl.ANY)],
        out_specs=(VMEM_SPEC,) * 3,
        scratch_shapes=[
            pltpu.VMEM((tok_rows, model_width), jnp.bfloat16),
            DMA((3,)),
            DMA((3,)),
            pltpu.VMEM((1, model_width), jnp.float32),
            pltpu.VMEM((tok_rows, 8), jnp.float32),
            pltpu.VMEM(flat_rows.shape, jnp.bfloat16),
            DMA(()),
            slots,
            slots,
            pltpu.VMEM((operands[1].shape[0], span_rows, 2 * head_dim), jnp.bfloat16),
            slots,
            slots,
            DMA((2, 2, st_count)),
            pltpu.VMEM((tok_rows, head_dim), jnp.bfloat16),
            pltpu.VMEM((tok_rows, head_dim), jnp.bfloat16),
            pltpu.VMEM((tok_rows, head_dim), jnp.bfloat16),
            pltpu.VMEM((tok_rows, 1), jnp.float32),
            pltpu.VMEM((tok_rows, 1), jnp.float32),
            pltpu.VMEM((tok_rows, head_dim), jnp.float32),
            pltpu.VMEM((heads_n, mix_dim, mix_dim), jnp.float32),
            pltpu.VMEM((per_block * span_rows, 2 * head_dim), jnp.bfloat16),
            pltpu.VMEM((rows, head_dim), jnp.bfloat16),
            pltpu.VMEM((rows, head_dim), jnp.bfloat16),
            pltpu.VMEM((model_width, head_dim), jnp.bfloat16),
            pltpu.VMEM((st_count, part, head_dim), jnp.bfloat16),
            DMA((st_count,)),
            DMA((st_count,)),
            *scatter_scratch(tok_chunks, tok_rows // tok_chunks, width),
            *scatter_scratch(row_chunks, rows // row_chunks, width),
        ],
        compiler_params=pltpu.CompilerParams(collective_id=1, has_side_effects=True),
        name="exchange_attend",
    )(*operands)


def request_slots(id_rows, pass_count):
    owners = id_rows // pass_count
    local_idx = id_rows % pass_count
    req_count = id_rows.shape[-1]
    req_order = jnp.arange(req_count, dtype=jnp.int32)
    earlier = (owners[..., :, None] == owners[..., None, :]) & (
        req_order[None, :] < req_order[:, None]
    )
    ranks = jnp.sum(earlier.astype(jnp.int32), axis=-1, dtype=jnp.int32)
    return (owners, local_idx, ranks)


def body(
    tokens,
    cotangent,
    mix_query,
    mix_key,
    mix_value,
    beta_pre,
    decay_pre,
    decay_rate,
    passages,
    passage_ids,
    query_weight,
    key_weight,
    value_weight,
    gate_weight,
):
    model_width = query_weight.shape[0]
    head_dim = query_weight.shape[1]
    pass_local = passages.shape[0]
    span_rows = passages.shape[1]
    blocks_n = passage_ids.shape[0]
    per_block = passage_ids.shape[1]
    req_count = blocks_n * per_block
    st_count = lax.axis_size("st")
    my_owner = lax.axis_index("st")
    cap_count = max(1, req_count // st_count)
    slot_total = st_count * cap_count
    req_order = jnp.arange(req_count, dtype=jnp.int32)
    flat_rows = passages.reshape(pass_local * span_rows, model_width)
    flat_ids = passage_ids.reshape(1, req_count)
    ids_padded = jnp.pad(flat_ids, ((0, 7), (0, -req_count % 128)))
    ids_all, key_low, packed = project_call(
        st_count, ids_padded, flat_rows, key_weight, value_weight
    )
    every_id = ids_all[:, 0, :req_count]
    packed = packed.reshape(pass_local, span_rows, 2 * head_dim)
    all_owner, all_local, all_rank = request_slots(every_id, pass_local)
    cap_iota = jnp.arange(cap_count, dtype=jnp.int32)
    wanted = (all_owner == my_owner)[:, None, :] & (all_rank[:, None, :] == cap_iota[None, :, None])
    slot_used = jnp.any(wanted, axis=-1)
    slot_local = jnp.sum(jnp.where(wanted, all_local[:, None, :], 0), axis=-1, dtype=jnp.int32)
    own_owner, _, own_rank = request_slots(passage_ids.reshape(req_count), pass_local)
    slot_of = own_owner * cap_count + own_rank
    slot_match = slot_of[None, :] == jnp.arange(slot_total, dtype=jnp.int32)[:, None]
    slot_req = jnp.sum(jnp.where(slot_match, req_order[None, :], 0), axis=-1, dtype=jnp.int32)
    slot_row = jnp.where(slot_used, slot_local * span_rows, -span_rows).reshape(slot_total, 1)
    code = (slot_row + jnp.arange(span_rows, dtype=jnp.int32)[None, :]).reshape(1, -1)
    token_grad, passage_grad, key_weight_grad = main_call(
        st_count,
        cap_count,
        per_block,
        span_rows,
        slot_local.reshape(slot_total),
        slot_of,
        slot_req,
        decay_rate,
        code,
        tokens,
        packed,
        key_low,
        cotangent,
        mix_query,
        mix_key,
        mix_value,
        beta_pre,
        decay_pre,
        query_weight,
        gate_weight,
        key_weight,
        value_weight,
        flat_rows,
    )
    token_grad, passage_grad, key_weight_grad = settle_call(
        token_grad, passage_grad, key_weight_grad
    )
    passage_grad = passage_grad.reshape(pass_local, span_rows, -1)
    return (token_grad, passage_grad, key_weight_grad)


def solution(mesh):
    placed = (
        P("st", "tp"),
        P("st", "tp"),
        P("st", "tp"),
        P("st", "tp"),
        P("st", "tp"),
        P("tp", "st"),
        P("tp", "st"),
        P("tp"),
        P("st", None, None),
        P("st", None),
        P(None, "tp"),
        P(None, "tp"),
        P(None, "tp"),
        P("tp", None),
    )
    return jax.shard_map(
        body,
        mesh=mesh,
        in_specs=placed,
        out_specs=(P("st", "tp"), P("st", None, "tp"), P("st", "tp")),
        check_vma=False,
    )
```

profile of v0, /device:TPU:1, one launch (start us, length us, event | category | flops | bytes accessed | tf_op | source)
XLA Modules:
  0.0 317.8 jit_solution(7842870767105707465)
XLA Ops:
  0.6 0.8 copy.29
  1.4 0.1 reshape.179
  1.5 0.1 reshape.177
  1.6 0.2 convert_reduce_fusion.1
  1.8 0.0 copy-start.1
  1.8 0.6 select_reduce_fusion.request_ref
  2.4 0.6 pad.4.ids_ref
  3.0 23.1 %ids_project.1 = (s32[64,8,128]{2,1,0:T(8,128)}, bf16[1024,256]{1,0:T(8,128)(2,1)}, bf16[1024,512]{1,0:T(8,128)(2,1)}) custom-call(s32[8,128]{1,0:T(8,128)} %pad.4.ids_ref, bf16[1024,2048]{1,0:T(8,128)(2,1)} %bitcast.10, bf16[2048,256]{1,0:T(8,128)(2,1)} %kw_ref.3, bf16[2048,256]{1,0:T(8,128)(2,1)} %vw_ref.3), custom_call_target="tpu_custom_call" | custom-call | tf_op jit(solution)/shard_map/ids_project/pallas_call | solution.py:190
  26.1 1.0 slice.3
  27.1 0.1 copy.34
  27.2 0.1 copy.35
  27.3 0.2 convert_reduce_fusion
  27.5 0.1 copy.36
  27.6 0.1 fusion.7
  27.7 0.1 fusion.2.local_ref
  27.8 0.0 copy-start
  27.8 0.1 iota_add_fusion
  27.9 0.7 add.60.code_ref
  28.6 0.0 copy-done.1
  28.6 0.0 copy-done
  28.6 286.7 %exchange_attend.1 = (bf16[384,512]{1,0:T(8,128)(2,1)}, bf16[1024,512]{1,0:T(8,128)(2,1)}, f32[32,256]{1,0:T(8,128)}) custom-call(s32[64]{0:T(128)} %copy-done, s32[24]{0:T(128)} %copy-done.1, s32[64]{0:T(128)} %select_reduce_fusion.request_ref, f32[2]{0:T(128)} %rate_ref.1, s32[1,4096]{1,0:T(1,128)} %add.60.code_ref, bf16[384,512]{1,0:T(8,128)(2,1)} %own_ref.1, ...), custom_call_target="tpu_custom_call" | custom-call | tf_op jit(solution)/shard_map/exchange_attend/pallas_call | solution.py:592
  315.3 2.5 settle.1
  (6 shorter events, 0.1 us)
Async XLA Ops:
  1.8 26.8 %copy-start.1 = (s32[24]{0:T(128)}, s32[24]{0:T(128)S(1)}, u32[]{:S(2)}) copy-start(s32[24]{0:T(128)S(1)} %fusion.8.slot_ref) | copy-start | bytes 292
  27.8 0.8 copy-start
where the time goes:
time: 324 us; the launch traced here: 318 us
  Pallas kernels  312 us (96%)
  local copies, waits for them, and re-layouts  3.41 us (1%)
    pallas_call x1, Pallas kernels, main_call(): pl.pallas_call(functools.partial(main_kernel, st_count, (cap, per_block,...  287 us
    pallas_call x1, Pallas kernels, project_call(): pl.pallas_call(functools.partial(project_kernel, st_count), out_shape=(ja...  23.1 us

commit v1 on v0

v1 whole, which is shorter than its diff:
```python
import functools

import jax
import jax.numpy as jnp
from jax import lax
from jax.experimental import pallas as pl
from jax.experimental.pallas import tpu as pltpu
from jax.sharding import PartitionSpec as P

SPAN = 64
BLOCK = 64
NORM_FLOOR = 1.0
SCORE_GAIN = 4.0
HIGHEST = lax.Precision.HIGHEST
CONTRACT_LAST = (((1,), (1,)), ((), ()))
CONTRACT_FIRST = (((0,), (0,)), ((), ()))
F32, BF16 = jnp.float32, jnp.bfloat16

MESH = pl.DeviceIdType.MESH
VMEM_SPEC = pl.BlockSpec(memory_space=pltpu.VMEM)
ANY_SPEC = pl.BlockSpec(memory_space=pl.ANY)
SMEM_SPEC = pl.BlockSpec(memory_space=pltpu.SMEM)
DMA = pltpu.SemaphoreType.DMA

ZN, YN, CN, XN = 8, 4, 2, 4
ROW = 128


def settle_kernel(*refs):
    count = len(refs) // 2
    for source, target in zip(refs[:count], refs[count:]):
        target[...] = source[...]


def settle_call(*arrays):
    return pl.pallas_call(
        settle_kernel,
        out_shape=tuple(jax.ShapeDtypeStruct(x.shape, x.dtype) for x in arrays),
        in_specs=[VMEM_SPEC] * len(arrays),
        out_specs=(VMEM_SPEC,) * len(arrays),
        name="settle",
    )(*arrays)


def exact_dot(left, right, dims=(((1,), (0,)), ((), ()))):
    return lax.dot_general(left, right, dims, precision=HIGHEST, preferred_element_type=F32)


def low_dot(left, right, dims=(((1,), (0,)), ((), ()))):
    return lax.dot_general(left, right, dims, preferred_element_type=F32)


def mixer_span(queries, keys_in, values_in, strength, log_decay, state):
    span = queries.shape[0]
    row_at = lax.broadcasted_iota(jnp.int32, (span, span), 0)
    col_at = lax.broadcasted_iota(jnp.int32, (span, span), 1)
    inclusive = row_at >= col_at
    unit_eye = jnp.where(row_at == col_at, 1.0, 0.0)
    decay_row = jnp.sum(unit_eye * log_decay, axis=0, keepdims=True)
    cum_row = jnp.sum(jnp.where(row_at <= col_at, log_decay, 0.0), axis=0, keepdims=True)
    cum_col = jnp.sum(jnp.where(inclusive, decay_row, 0.0), axis=1, keepdims=True)
    total = jnp.sum(log_decay, axis=0, keepdims=True)
    decay_map = jnp.exp(jnp.where(inclusive, cum_col - cum_row, -1e30))
    queries = (
        queries
        * lax.rsqrt(jnp.sum(queries * queries, axis=-1, keepdims=True) + NORM_FLOOR)
        * queries.shape[-1] ** (-0.5)
    )
    keys_in = keys_in * lax.rsqrt(jnp.sum(keys_in * keys_in, axis=-1, keepdims=True) + NORM_FLOOR)
    power = jnp.where(
        row_at > col_at, strength * exact_dot(keys_in, keys_in, CONTRACT_LAST) * decay_map, 0.0
    )
    inverse = unit_eye - power
    for _ in range(span.bit_length() - 2):
        power = exact_dot(power, power)
        inverse = exact_dot(inverse, unit_eye + power)
    attend = exact_dot(queries, keys_in, CONTRACT_LAST) * decay_map
    fresh = exact_dot(inverse, values_in * strength)
    correction = exact_dot(inverse, keys_in * (strength * jnp.exp(cum_col)))
    new_values = fresh - exact_dot(correction, state)
    output = exact_dot(queries * jnp.exp(cum_col), state) + exact_dot(attend, new_values)
    state = state * jnp.exp(total) + exact_dot(
        keys_in * jnp.exp(total - cum_col), new_values, CONTRACT_FIRST
    )
    return output, state


def scratch_spec(tok_n, rows_n, width, head, heads_n, mix_dim):
    model = width * XN
    slab = YN * CN
    passes = rows_n // BLOCK
    chunks = rows_n // ROW
    half = chunks // 2
    part = model // (ZN * slab)
    keys = slab * BLOCK
    vmem = dict(
        rows_v=((rows_n, model), BF16),
        kw=((model, head), BF16),
        vw=((model, head), BF16),
        qw=((model, head), BF16),
        tok4=((XN, tok_n, width), BF16),
        kv=((slab * passes, BLOCK, 2 * head), BF16),
        qc=((ZN, 2, tok_n, head), BF16),
        gates=((ZN, 8, tok_n), F32),
        mq=((tok_n, head), BF16),
        mk=((tok_n, head), BF16),
        mv=((tok_n, head), BF16),
        ids_all=((CN, ZN, 8, 128), jnp.int32),
        tab_v=((2, CN * ZN, 128), jnp.int32),
        code=((YN, CN, 8, ZN * BLOCK), jnp.int32),
        turned=((tok_n, 8), F32),
        mixed=((tok_n, head), F32),
        states=((heads_n, mix_dim, mix_dim), F32),
        key_low=((rows_n, head), BF16),
        query_low=((tok_n, head), BF16),
        query_grad=((tok_n, head), BF16),
        gate_grad=((tok_n, 1), F32),
        gw=((1, model), F32),
        kvr=((keys, 2 * head), BF16),
        e_buf=((ZN, keys, tok_n), F32),
        g_buf=((keys, tok_n), F32),
        sg=((keys, tok_n), BF16),
        pg=((keys, tok_n), BF16),
        zt=((ZN, 2, tok_n), F32),
        zt_r=((ZN, ZN, 2, tok_n), F32),
        terms=((YN, CN, ZN, BLOCK, 2 * head), BF16),
        term_r=((YN, ZN, BLOCK, 2 * head), BF16),
        qg=((ZN, tok_n, head), BF16),
        z_s=((2, ZN // 2, tok_n, head), BF16),
        z_r=((2, ZN // 2, tok_n, head), BF16),
        yf_s=((2, half, ROW, 2 * head), BF16),
        yf_r=((2, half, ROW, 2 * head), BF16),
        yd_s=((2, chunks, ROW, 2 * head), BF16),
        yd_r=((2, chunks, ROW, 2 * head), BF16),
        key_grad=((rows_n, head), BF16),
        value_grad=((rows_n, head), BF16),
        xf_s=((2, half, ROW, width), BF16),
        xf_r=((2, half, ROW, width), BF16),
        xd_s=((2, chunks, ROW, width), BF16),
        xd_r=((2, chunks, ROW, width), BF16),
        tf_s=((2, tok_n // 2, width), BF16),
        tf_r=((2, tok_n // 2, width), BF16),
        td_s=((2, 2, tok_n // 2, width), BF16),
        td_r=((2, 2, tok_n // 2, width), BF16),
        wbuf=((CN, YN, ZN, part, head), BF16),
        wc_r=((YN, ZN, part, head), BF16),
        w1=((YN, ZN, part, head), BF16),
        wy_r=((YN, ZN, part, head), BF16),
        w2=((ZN, part, head), BF16),
        wz_r=((ZN, part, head), BF16),
    )
    sems = dict(
        load=(16,),
        idsem=(2, CN, ZN),
        tokx=(2, 2, 2),
        cotz=(2, ZN // 2, 2),
        qz=(2, ZN // 2, 2),
        gz=(2, ZN // 2, 2),
        kvy=(2, 2, 2, 4),
        kvd=(2, YN, 4),
        zts=(2, ZN),
        ters=(2, YN),
        zrs=(2, 2, ZN // 2),
        yfs=(2, 2, half),
        yds=(2, 2, chunks),
        xfs=(2, 2, half),
        xds=(2, 2, chunks),
        tfs=(2, 2),
        tds=(2, 2, 2),
        wcs=(2,),
        wys=(2, YN),
        wzs=(2, ZN),
    )
    return vmem, sems


def fused_kernel(names, *refs):
    r = dict(zip(names, refs))

    def get(*keys):
        return [r[k] for k in keys]

    rate, ids, gate_w, beta, decay = get("rate", "ids", "gate_w", "beta", "decay")
    tok_out, out_ref, weight_ref = get("tok_out", "out_ref", "weight_ref")
    rows_v, kw, vw, qw, tok4, kv, qc, gates = get(
        "rows_v", "kw", "vw", "qw", "tok4", "kv", "qc", "gates"
    )
    tab_v, tab_s, code = get("tab_v", "tab_s", "code")
    kvr, e_buf, g_buf, sg, pg, zt, zt_r = get("kvr", "e_buf", "g_buf", "sg", "pg", "zt", "zt_r")
    terms, term_r, qg, z_s, z_r = get("terms", "term_r", "qg", "z_s", "z_r")
    key_low, key_grad, value_grad = get("key_low", "key_grad", "value_grad")
    query_low, query_grad, gate_grad = get("query_low", "query_grad", "gate_grad")
    turned, mixed, states = get("turned", "mixed", "states")
    gw = r["gw"]

    rows_n, model = rows_v.shape
    head = kw.shape[1]
    tok_n, width = tok_out.shape
    heads_n = beta.shape[0]
    mix_dim = head // heads_n
    slab = YN * CN
    passes = rows_n // BLOCK
    chunks = rows_n // ROW
    half = chunks // 2
    per_dev = tok_n // BLOCK
    score_scale = SCORE_GAIN * head ** (-0.5)

    st = lax.axis_index("st")
    x = lax.axis_index("tp")
    c = lax.rem(st, CN)
    y = lax.rem(st // CN, YN)
    z = st // slab
    other = 1 - c

    def at(zi, yi, ci):
        return (zi * YN + yi) * CN + ci

    def step(value, by, n):
        return lax.rem(value + (by % n), n)

    xs = [step(x, i, XN) for i in range(XN)]
    ys = [step(y, i, YN) for i in range(YN)]
    zs = [step(z, i, ZN) for i in range(ZN)]
    partner = at(z, y, other)
    x_to = (xs[1], xs[XN - 1])
    y_to = (at(z, ys[1], c), at(z, ys[YN - 1], c))
    z_to = (at(zs[1], y, c), at(zs[ZN - 1], y, c))

    started = []

    def remote(src, dst, sem, index, st_id=None, tp_id=None):
        sems = r[sem]
        device = {}
        if st_id is not None:
            device["st"] = st_id
        if tp_id is not None:
            device["tp"] = tp_id
        return pltpu.make_async_remote_copy(
            src_ref=src,
            dst_ref=dst,
            send_sem=sems.at[(0, *index)],
            recv_sem=sems.at[(1, *index)],
            device_id=device,
            device_id_type=MESH,
        )

    def go(copy):
        copy.start()
        started.append(copy)

    loads = {}

    def load(key, src, dst):
        loads[key] = pltpu.make_async_copy(src, dst, r["load"].at[len(loads)])
        loads[key].start()

    load("cot", r["cot_h"], qc.at[z, 1])
    load("tok", r["tok_h"], tok4.at[x])
    load("kw", r["kw_h"], kw)
    load("vw", r["vw_h"], vw)
    proj_rows = rows_n // 4
    proj_order = (0, 2, 1, 3)
    for k in proj_order:
        here = pl.ds(k * proj_rows, proj_rows)
        load(("rows", k), r["rows_h"].at[here, :], rows_v.at[here, :])
    load("mq", r["mq_h"], r["mq"])
    load("mk", r["mk_h"], r["mk"])
    load("mv", r["mv_h"], r["mv"])
    load("qw", r["qw_h"], qw)

    barrier = pltpu.get_barrier_semaphore()
    greeted = 0
    for target in x_to:
        pl.semaphore_signal(barrier, inc=1, device_id={"tp": target}, device_id_type=MESH)
        greeted += 1
    friends = [partner] + [at(z, ys[d], c) for d in range(1, YN)]
    friends += [at(zs[d], y, ci) for d in range(1, ZN) for ci in (c, other)]
    for target in friends:
        pl.semaphore_signal(barrier, inc=1, device_id={"st": target}, device_id_type=MESH)
        greeted += 1
    pl.semaphore_wait(barrier, greeted)

    t_half = tok_n // 2
    half_rows = (pl.ds(0, t_half), pl.ds(t_half, t_half))

    def cot_copy(hop, d):
        source = zs[(1 - hop) % ZN] if d == 0 else zs[(hop - 1) % ZN]
        ref = qc.at[source, 1]
        if hop == ZN // 2:
            ref = qc.at[source, 1, half_rows[d]]
        return remote(ref, ref, "cotz", (hop - 1, d), st_id=z_to[d])

    def q_copies(hop, d):
        source = zs[(1 - hop) % ZN] if d == 0 else zs[(hop - 1) % ZN]
        ref = qc.at[source, 0]
        if hop == ZN // 2:
            ref = qc.at[source, 0, half_rows[d]]
        copies = [remote(ref, ref, "qz", (hop - 1, d), st_id=z_to[d])]
        if hop < ZN // 2 or d == 0:
            copies.append(
                remote(gates.at[source], gates.at[source], "gz", (hop - 1, d), st_id=z_to[d])
            )
        return copies

    def tok_copy(hop, d):
        if hop == 1:
            ref = tok4.at[x]
        else:
            ref = tok4.at[xs[XN - 1] if d == 0 else xs[1], half_rows[d]]
        return remote(ref, ref, "tokx", (hop - 1, d), tp_id=x_to[d])

    loads["tok"].wait()
    for d in range(2):
        go(tok_copy(1, d))
    loads["cot"].wait()
    for d in range(2):
        go(cot_copy(1, d))

    def ids_copy(dc, dz):
        return remote(
            ids, r["ids_all"].at[c, z], "idsem", (dc, dz), st_id=at(zs[dz], y, other if dc else c)
        )

    id_peers = [(dc, dz) for dz in range(ZN) for dc in range(CN) if (dc, dz) != (0, 0)]
    for dc, dz in id_peers:
        go(ids_copy(dc, dz))
    r["ids_all"][c, z] = ids[...]

    per_chunk = proj_rows // BLOCK

    def kv_piece(yi, ci, k):
        return kv.at[pl.ds((yi * CN + ci) * passes + k * per_chunk, per_chunk)]

    def kv_copy(hop, d, k):
        yi = y if hop == 1 else (ys[YN - 1] if d == 0 else ys[1])
        ref = kv_piece(yi, c, k)
        return remote(ref, ref, "kvy", (hop - 1, d, k), st_id=y_to[d])

    def kv_across(rel, k):
        ref = kv_piece(ys[rel], c, k)
        return remote(ref, ref, "kvd", (rel, k), st_id=partner)

    loads["kw"].wait()
    loads["vw"].wait()
    for k in proj_order:
        loads[("rows", k)].wait()
        here = pl.ds(k * proj_rows, proj_rows)
        block = rows_v[here, :]
        low = low_dot(block, kw[...]).astype(BF16)
        key_low[here, :] = low
        low = low.astype(F32)
        scale = lax.rsqrt(jnp.mean(low * low, axis=-1, keepdims=True) + NORM_FLOOR)
        first = (y * CN + c) * passes + k * per_chunk
        kv[pl.ds(first, per_chunk), :, :head] = (
            (low * scale).astype(BF16).reshape(per_chunk, BLOCK, head)
        )
        kv[pl.ds(first, per_chunk), :, head:] = (
            low_dot(block, vw[...]).astype(BF16).reshape(per_chunk, BLOCK, head)
        )
        for d in range(2):
            go(kv_copy(1, d, k))
        go(kv_across(0, k))

    for dc, dz in id_peers:
        ids_copy(dc, dz).wait_recv()
    every = jnp.concatenate(
        [r["ids_all"][ci, zi, 0:1, :] for ci in range(CN) for zi in range(ZN)], axis=0
    )
    lane = lax.broadcasted_iota(jnp.int32, (CN * ZN, 128), 1)
    loc_tab = jnp.zeros((CN * ZN, 128), jnp.int32)
    blk_tab = jnp.zeros((CN * ZN, 128), jnp.int32)
    owner = lax.shift_right_logical(every, 4)
    local = every & (passes - 1)
    for o in range(slab):
        match = (owner == z * slab + o) & (lane < per_dev * 4)
        loc = jnp.sum(jnp.where(match, local, 0), axis=1, keepdims=True)
        blk = jnp.sum(
            jnp.where(match, lax.shift_right_logical(lane, 2) + 1, 0), axis=1, keepdims=True
        )
        loc_tab = jnp.where(lane == o, jnp.minimum(loc, passes - 1), loc_tab)
        blk_tab = jnp.where(lane == o, blk - 1, blk_tab)
    tab_v[0] = loc_tab
    tab_v[1] = blk_tab
    tab_copy = pltpu.make_async_copy(tab_v, tab_s, r["load"].at[len(loads)])
    tab_copy.start()

    gw[...] = gate_w[...].astype(F32)
    turned[...] = jnp.transpose(
        jnp.concatenate(
            [beta[...], decay[...], jnp.zeros((8 - 2 * heads_n, tok_n), F32)], axis=0
        )
    )
    states[...] = jnp.zeros_like(states)
    for key in ("mq", "mk", "mv", "qw"):
        loads[key].wait()

    def mix(b):
        here = pl.ds(pl.multiple_of(b * SPAN, SPAN), SPAN)
        for m in range(heads_n):
            cols = pl.ds(m * mix_dim, mix_dim)
            raw = turned[here, heads_n + m : heads_n + m + 1]
            softplus = jnp.maximum(raw, 0.0) + jnp.log1p(jnp.exp(-jnp.abs(raw)))
            mixed[here, cols], states[m] = mixer_span(
                r["mq"][here, cols].astype(F32),
                r["mk"][here, cols].astype(F32),
                r["mv"][here, cols].astype(F32),
                jax.nn.sigmoid(turned[here, m : m + 1]),
                -rate[m] * softplus,
                states[m],
            )

    spans_n = tok_n // SPAN

    def cot_pass(hop):
        for d in range(2):
            cot_copy(hop - 1, d).wait_recv()
            go(cot_copy(hop, d))

    def q_pass(hop):
        for d in range(2):
            for copy in q_copies(hop - 1, d):
                copy.wait_recv()
            for copy in q_copies(hop, d):
                go(copy)

    def kv_pass(k):
        for d, rel in ((0, YN - 1), (1, 1)):
            kv_copy(1, d, k).wait_recv()
            if (k < 2) == (d == 0):
                go(kv_copy(2, d, k))
            go(kv_across(rel, k))

    pl.loop(0, 1)(mix)
    cot_pass(2)
    for d in range(2):
        tok_copy(1, d).wait_recv()
        go(tok_copy(2, d))
    pl.loop(1, 2)(mix)
    for d in range(2):
        tok_copy(2, d).wait_recv()

    gate_rows = jnp.broadcast_to(gate_w[...], (16, model))
    logit = low_dot(gate_rows[:, :width], tok4[0], CONTRACT_LAST)
    for i in range(1, XN):
        logit += low_dot(gate_rows[:, i * width : (i + 1) * width], tok4[i], CONTRACT_LAST)
    gates[z] = jax.nn.sigmoid(logit[:8])

    @pl.loop(0, tok_n // ROW)
    def _(k):
        here = pl.ds(pl.multiple_of(k * ROW, ROW), ROW)
        low = low_dot(tok4[0, here, :], qw[pl.ds(0, width), :])
        for i in range(1, XN):
            low += low_dot(tok4[i, here, :], qw[pl.ds(i * width, width), :])
        low = low.astype(BF16)
        query_low[here, :] = low
        low = low.astype(F32)
        scale = lax.rsqrt(jnp.mean(low * low, axis=-1, keepdims=True) + NORM_FLOOR)
        qc[z, 0, here, :] = (low * scale).astype(BF16)

    for d in range(2):
        for copy in q_copies(1, d):
            go(copy)
    cot_pass(3)
    kv_pass(0)
    pl.loop(2, 4)(mix)
    kv_pass(2)
    cot_pass(4)
    q_pass(2)
    pl.loop(4, spans_n)(mix)
    kv_pass(1)
    q_pass(3)
    kv_pass(3)
    q_pass(4)
    tab_copy.wait()
    lane_of = lax.broadcasted_iota(jnp.int32, (8, ZN * BLOCK), 1)
    for yi in range(YN):
        for which, ci in ((0, c), (1, other)):
            start = jnp.full((8, ZN * BLOCK), -1000000, jnp.int32)
            for zi in range(ZN):
                row = ci * ZN + zi
                base = jnp.where(
                    tab_s[1, row, yi * CN + c] >= 0,
                    tab_s[0, row, yi * CN + c] * BLOCK,
                    -1000000,
                )
                start = jnp.where(lax.shift_right_logical(lane_of, 6) == zi, base, start)
            code[yi, which] = start + (lane_of & (BLOCK - 1))
    for d in range(2):
        cot_copy(ZN // 2, d).wait_recv()
        for copy in q_copies(ZN // 2, d):
            copy.wait_recv()
    for d, k in ((0, 0), (1, 2), (0, 1), (1, 3)):
        kv_copy(2, d, k).wait_recv()
        go(kv_across(2, k))
    for rel in range(YN):
        for k in range(4):
            kv_across(rel, k).wait_recv()

    tok_block = lax.shift_right_logical(lax.broadcasted_iota(jnp.int32, (BLOCK, tok_n), 1), 6)
    key_halves = [pl.ds(i * ROW * 2, ROW * 2) for i in range(slab * BLOCK // (2 * ROW))]

    def gather(reader):
        for o in range(slab):
            local_at = jnp.clip(tab_s[0, c * ZN + reader, o], 0, passes - 1)
            kvr[pl.ds(o * BLOCK, BLOCK), :] = kv[o * passes + local_at]

    @pl.loop(0, ZN)
    def _(reader):
        gather(reader)
        for part in key_halves:
            e_buf[reader, part, :] = low_dot(kvr[part, :head], qc[reader, 0], CONTRACT_LAST)
            g_buf[part, :] = low_dot(kvr[part, head:], qc[reader, 1], CONTRACT_LAST)
        total = jnp.zeros((1, tok_n), F32)
        product = jnp.zeros((1, tok_n), F32)
        for o in range(slab):
            here = pl.ds(o * BLOCK, BLOCK)
            mine = tok_block == tab_s[1, c * ZN + reader, o]
            e = jnp.where(mine, jnp.exp(e_buf[reader, here, :] * score_scale), 0.0)
            e_buf[reader, here, :] = e
            total += jnp.sum(e, axis=0, keepdims=True)
            product += jnp.sum(e * g_buf[here, :], axis=0, keepdims=True)
        zt[reader, 0:1, :] = total
        zt[reader, 1:2, :] = product * gates[reader, 0:1, :]

    def zt_copy(d):
        return remote(zt, zt_r.at[d], "zts", (d,), st_id=at(zs[d], y, c))

    for d in range(1, ZN):
        go(zt_copy(d))
    for d in range(1, ZN):
        zt_copy(d).wait_recv()

    def summed(reader):
        both = zt[reader]
        for d in range(1, ZN):
            both += zt_r[d, reader]
        return both[0:1, :], both[1:2, :]

    @pl.loop(0, ZN)
    def _(i):
        reader = lax.rem(z + jnp.where(lax.rem(i, 2) == 1, 4 - (i + 1) // 2, 4 + i // 2), ZN)
        total, product = summed(reader)
        inverse = 1.0 / total
        mean = product * inverse
        gate = gates[reader, 0:1, :]
        gather(reader)
        for part in key_halves:
            g_buf[part, :] = low_dot(kvr[part, head:], qc[reader, 1], CONTRACT_LAST)
        for o in range(slab):
            here = pl.ds(o * BLOCK, BLOCK)
            probs = e_buf[reader, here, :] * inverse
            sg[here, :] = (probs * (g_buf[here, :] * gate - mean)).astype(BF16)
            pg[here, :] = (probs * gate).astype(BF16)
        for n, part in enumerate(key_halves):
            key_term = (low_dot(sg[part, :], qc[reader, 0]) * score_scale).astype(BF16)
            value_term = low_dot(pg[part, :], qc[reader, 1]).astype(BF16)
            for k in range(2 * ROW // BLOCK):
                o = n * (2 * ROW // BLOCK) + k
                piece = slice(k * BLOCK, (k + 1) * BLOCK)
                terms[o // CN, o % CN, reader, :, :head] = key_term[piece]
                terms[o // CN, o % CN, reader, :, head:] = value_term[piece]
        qg[reader] = (low_dot(sg[...], kvr[:, :head], CONTRACT_FIRST) * score_scale).astype(BF16)

    def z_copy(hop, d):
        if hop == 1:
            src = qg.at[zs[ZN // 2], half_rows[d]]
            dst = z_r.at[d, 0, half_rows[d]]
        else:
            src = z_s.at[d, hop - 1]
            dst = z_r.at[d, hop - 1]
        return remote(src, dst, "zrs", (d, hop - 1), st_id=z_to[d])

    def z_pass(hop):
        for d in range(2):
            z_copy(hop - 1, d).wait_recv()
            away = ZN // 2 + 1 - hop
            target = zs[away] if d == 0 else zs[(-away) % ZN]
            if hop == 2:
                mid, rest = half_rows[d], half_rows[1 - d]
                z_s[d, hop - 1, mid, :] = (
                    qg[target, mid, :].astype(F32) + z_r[d, 0, mid, :].astype(F32)
                ).astype(BF16)
                z_s[d, hop - 1, rest, :] = qg[target, rest, :]
            else:
                z_s[d, hop - 1] = (
                    qg[target].astype(F32) + z_r[d, hop - 2].astype(F32)
                ).astype(BF16)
            go(z_copy(hop, d))

    def term_copy(rel):
        return remote(
            terms.at[ys[rel], other], term_r.at[ys[rel]], "ters", (rel,), st_id=partner
        )

    for rel in (2, 1, 3, 0):
        go(term_copy(rel))
    for d in range(2):
        go(z_copy(1, d))

    row_iota = lax.broadcasted_iota(jnp.int32, (ROW, ZN * BLOCK), 0)

    def pick(rel, q):
        yi = ys[rel]
        rows = row_iota + q * ROW
        ones = [
            jnp.where(rows == code[yi, which, 0:1, :], 1.0, 0.0).astype(BF16) for which in range(2)
        ]
        return low_dot(ones[0], terms[yi, c].reshape(ZN * BLOCK, 2 * head)) + low_dot(
            ones[1], term_r[yi].reshape(ZN * BLOCK, 2 * head)
        )

    yf_s, yf_r, yd_s, yd_r = get("yf_s", "yf_r", "yd_s", "yd_r")
    xf_s, xf_r, xd_s, xd_r = get("xf_s", "xf_r", "xd_s", "xd_r")

    def two_step(far_s, far_r, near_s, near_r, far_sem, near_sem, term, axis):
        def target(d):
            return {"st_id": y_to[d]} if axis == "y" else {"tp_id": x_to[d]}

        def far(d, j):
            return remote(far_s.at[d, j], far_r.at[d, j], far_sem, (d, j), **target(d))

        def near(d, q):
            return remote(near_s.at[d, q], near_r.at[d, q], near_sem, (d, q), **target(d))

        def send(j):
            for d in range(2):
                q = j + half * d
                far_s[d, j] = term(2, q).astype(BF16)
                go(far(d, j))
            for d in range(2):
                q = j + half * (1 - d)
                near_s[d, q] = term(1 if d == 0 else 3, q).astype(BF16)
                go(near(d, q))

        def forward(j):
            for d in range(2):
                q = j + half * d
                value = term(1 if d == 0 else 3, q)
                far(d, j).wait_recv()
                near_s[d, q] = (value + far_r[d, j].astype(F32)).astype(BF16)
                go(near(d, q))

        def final(q):
            value = term(0, q)
            for d in range(2):
                near(d, q).wait_recv()
            return value + near_r[0, q].astype(F32) + near_r[1, q].astype(F32)

        return send, forward, final

    y_send, y_forward, y_final = two_step(yf_s, yf_r, yd_s, yd_r, "yfs", "yds", pick, "y")

    def row_term(rel, q):
        here = pl.ds(q * ROW, ROW)
        cols = pl.ds(pl.multiple_of(xs[rel] * width, width), width)
        return low_dot(key_grad[here, :], kw[cols, :], CONTRACT_LAST) + low_dot(
            value_grad[here, :], vw[cols, :], CONTRACT_LAST
        )

    x_send, x_forward, x_final = two_step(xf_s, xf_r, xd_s, xd_r, "xfs", "xds", row_term, "x")

    def finish_rows(j):
        for q in (j, j + half):
            here = pl.ds(q * ROW, ROW)
            value = y_final(q)
            hat = value[:, :head]
            low = key_low[here, :].astype(F32)
            scale = lax.rsqrt(jnp.mean(low * low, axis=-1, keepdims=True) + NORM_FLOOR)
            key_grad[here, :] = (
                scale * hat
                - scale * scale * scale * low * jnp.mean(low * hat, axis=-1, keepdims=True)
            ).astype(BF16)
            value_grad[here, :] = value[:, head:].astype(BF16)

    def finish_out(j):
        for q in (j, j + half):
            out_ref[pl.ds(q * ROW, ROW), :] = x_final(q).astype(out_ref.dtype)

    for rel in (2, 1, 3):
        term_copy(rel).wait_recv()
    y_send(0)
    y_send(1)
    y_forward(0)
    z_pass(2)
    y_send(2)
    y_forward(1)
    z_pass(3)
    y_send(3)
    term_copy(0).wait_recv()
    finish_rows(0)
    x_send(0)
    z_pass(4)
    y_forward(2)
    x_forward(0)

    for d in range(2):
        z_copy(ZN // 2, d).wait_recv()
    total, product = summed(z)
    stack = jnp.transpose(
        jnp.concatenate(
            [gates[z, 0:1, :], product / total, jnp.zeros((6, tok_n), F32)], axis=0
        )
    )

    for k in range(tok_n // ROW):
        here = pl.ds(k * ROW, ROW)
        hat_grad = qg[z, here, :].astype(F32)
        for d in range(2):
            hat_grad += z_r[d, ZN // 2 - 1, here, :].astype(F32)
        low = query_low[here, :].astype(F32)
        scale = lax.rsqrt(jnp.mean(low * low, axis=-1, keepdims=True) + NORM_FLOOR)
        query_grad[here, :] = (
            scale * hat_grad
            - scale * scale * scale * low * jnp.mean(low * hat_grad, axis=-1, keepdims=True)
        ).astype(BF16)
        opened = stack[k * ROW : (k + 1) * ROW, 0:1]
        ratio = stack[k * ROW : (k + 1) * ROW, 1:2]
        along = jnp.sum(
            qc[z, 1, here, :].astype(F32) * mixed[here, :], axis=-1, keepdims=True
        )
        gate_grad[here, :] = (1.0 - opened) * (ratio - opened * along)

    tf_s, tf_r, td_s, td_r = get("tf_s", "tf_r", "td_s", "td_r")

    def token_term(rel, h):
        cols = pl.ds(pl.multiple_of(xs[rel] * width, width), width)
        here = half_rows[h]
        return (
            low_dot(query_grad[here, :], qw[cols, :], CONTRACT_LAST)
            + gate_grad[here, :] * gw[:, cols]
        )

    def t_far(d):
        return remote(tf_s.at[d], tf_r.at[d], "tfs", (d,), tp_id=x_to[d])

    def t_near(d, h):
        return remote(td_s.at[d, h], td_r.at[d, h], "tds", (d, h), tp_id=x_to[d])

    for d in range(2):
        tf_s[d] = token_term(2, d).astype(BF16)
        go(t_far(d))
    for d in range(2):
        td_s[d, 1 - d] = token_term(1 if d == 0 else 3, 1 - d).astype(BF16)
        go(t_near(d, 1 - d))

    finish_rows(1)
    x_send(1)
    y_forward(3)
    for d in range(2):
        value = token_term(1 if d == 0 else 3, d)
        t_far(d).wait_recv()
        td_s[d, d] = (value + tf_r[d].astype(F32)).astype(BF16)
        go(t_near(d, d))
    x_forward(1)
    finish_out(0)
    finish_rows(2)
    x_send(2)
    finish_rows(3)
    x_send(3)

    wbuf, wc_r, w1, wy_r, w2, wz_r = get("wbuf", "wc_r", "w1", "wy_r", "w2", "wz_r")
    part = weight_ref.shape[0]

    @pl.loop(0, ZN)
    def _(k):
        cols = pl.ds(pl.multiple_of(k * slab * part, slab * part), slab * part)
        tile = low_dot(rows_v[:, cols], key_grad[...], CONTRACT_FIRST).astype(BF16)
        for o in range(slab):
            wbuf[o % CN, o // CN, k] = tile[o * part : (o + 1) * part]

    wc_copy = remote(wbuf.at[other], wc_r, "wcs", (), st_id=partner)
    go(wc_copy)
    x_forward(2)
    wc_copy.wait_recv()
    for yi in range(YN):
        w1[yi] = (wbuf[c, yi].astype(F32) + wc_r[yi].astype(F32)).astype(BF16)

    def wy_copy(d):
        return remote(w1.at[ys[d]], wy_r.at[d], "wys", (d,), st_id=at(z, ys[d], c))

    def wz_copy(d):
        return remote(w2.at[zs[d]], wz_r.at[d], "wzs", (d,), st_id=at(zs[d], y, c))

    for d in (2, 1, 3):
        go(wy_copy(d))
    finish_out(1)
    for d in range(1, YN):
        wy_copy(d).wait_recv()
    gathered = w1[y].astype(F32)
    for d in range(1, YN):
        gathered += wy_r[d].astype(F32)
    w2[...] = gathered.astype(BF16)
    for d in (4, 3, 5, 2, 6, 1, 7):
        go(wz_copy(d))
    x_forward(3)
    for h in range(2):
        value = token_term(0, h)
        for d in range(2):
            t_near(d, h).wait_recv()
        tok_out[half_rows[h], :] = (
            value + td_r[0, h].astype(F32) + td_r[1, h].astype(F32)
        ).astype(tok_out.dtype)
    finish_out(2)
    for d in range(1, ZN):
        wz_copy(d).wait_recv()
    weight = w2[z].astype(F32)
    for d in range(1, ZN):
        weight += wz_r[d].astype(F32)
    weight_ref[...] = weight
    finish_out(3)
    for copy in started:
        copy.wait_send()


def fused_call(rate, ids, gate_w, beta, decay, tok, cot, mq, mk, mv, qw, kw, vw, rows):
    tok_n, width = tok.shape
    rows_n, model = rows.shape
    head = kw.shape[1]
    heads_n = beta.shape[0]
    vmem, sems = scratch_spec(tok_n, rows_n, width, head, heads_n, head // heads_n)
    part = model // (ZN * YN * CN)
    ins = ["rate", "ids", "gate_w", "beta", "decay"]
    ins += ["tok_h", "cot_h", "mq_h", "mk_h", "mv_h", "qw_h", "kw_h", "vw_h", "rows_h"]
    names = ins + ["tok_out", "out_ref", "weight_ref"] + list(vmem) + ["tab_s"] + list(sems)
    return pl.pallas_call(
        functools.partial(fused_kernel, names),
        out_shape=(
            jax.ShapeDtypeStruct((tok_n, width), BF16),
            jax.ShapeDtypeStruct((rows_n, width), BF16),
            jax.ShapeDtypeStruct((part, head), F32),
        ),
        in_specs=[SMEM_SPEC] + [VMEM_SPEC] * 4 + [ANY_SPEC] * 9,
        out_specs=(VMEM_SPEC,) * 3,
        scratch_shapes=[pltpu.VMEM(*v) for v in vmem.values()]
        + [pltpu.SMEM((2, CN * ZN, 128), jnp.int32)]
        + [DMA(s) for s in sems.values()],
        compiler_params=pltpu.CompilerParams(
            collective_id=0, has_side_effects=True, vmem_limit_bytes=67043328
        ),
        name="fused",
    )(rate, ids, gate_w, beta, decay, tok, cot, mq, mk, mv, qw, kw, vw, rows)


def body(
    tokens,
    cotangent,
    mix_query,
    mix_key,
    mix_value,
    beta_pre,
    decay_pre,
    decay_rate,
    passages,
    passage_ids,
    query_weight,
    key_weight,
    value_weight,
    gate_weight,
):
    pass_local, span_rows, model_width = passages.shape
    flat_rows = passages.reshape(pass_local * span_rows, model_width)
    req_count = passage_ids.size
    ids = jnp.pad(passage_ids.reshape(1, req_count), ((0, 7), (0, -req_count % 128)))
    token_grad, passage_grad, key_weight_grad = fused_call(
        decay_rate,
        ids,
        gate_weight,
        beta_pre,
        decay_pre,
        tokens,
        cotangent,
        mix_query,
        mix_key,
        mix_value,
        query_weight,
        key_weight,
        value_weight,
        flat_rows,
    )
    token_grad, passage_grad, key_weight_grad = settle_call(
        token_grad, passage_grad, key_weight_grad
    )
    return (token_grad, passage_grad.reshape(pass_local, span_rows, -1), key_weight_grad)


def solution(mesh):
    placed = (
        P("st", "tp"),
        P("st", "tp"),
        P("st", "tp"),
        P("st", "tp"),
        P("st", "tp"),
        P("tp", "st"),
        P("tp", "st"),
        P("tp"),
        P("st", None, None),
        P("st", None),
        P(None, "tp"),
        P(None, "tp"),
        P(None, "tp"),
        P("tp", None),
    )
    return jax.shard_map(
        body,
        mesh=mesh,
        in_specs=placed,
        out_specs=(P("st", "tp"), P("st", None, "tp"), P("st", "tp")),
        check_vma=False,
    )
```

time: 324 us -> 156 us (0.48); the launches traced: 318 us -> 155 us
  Pallas kernels: 312 us -> 153 us
    pallas_call x2 -> x1, Pallas kernels: 310 us -> 151 us  [fused_call(): pl.pallas_call(functools.partial(fused_kernel, names), out_shape=(jax.Sha...]
where the time goes in v1:
time: 156 us; the launch traced here: 155 us
  Pallas kernels  153 us (98%)
    pallas_call x1, Pallas kernels, fused_call(): pl.pallas_call(functools.partial(fused_kernel, names), out_shape=(jax.Sha...  151 us

profile of v1, /device:TPU:1, one launch (start us, length us, event | category | flops | bytes accessed | tf_op | source)
XLA Modules:
  0.0 155.1 jit_solution(4964026309637278402)
XLA Ops:
  0.6 0.8 copy.18
  1.4 0.1 reshape.15
  1.5 0.6 pad.4.refs_1_
  2.1 150.5 %fused.1 = (bf16[384,512]{1,0:T(8,128)(2,1)}, bf16[1024,512]{1,0:T(8,128)(2,1)}, f32[32,256]{1,0:T(8,128)}) custom-call(f32[2]{0:T(128)} %refs_0_.1, s32[8,128]{1,0:T(8,128)} %pad.4.refs_1_, bf16[1,2048]{1,0:T(2,128)(2,1)} %refs_2_.1, f32[2,384]{1,0:T(2,128)} %refs_3_.1, f32[2,384]{1,0:T(2,128)} %refs_4_.1, bf16[384,512]{1,0:T(8,128)(2,1)} %refs_5_.1, ...), custom_call_target="tpu_custom_call" | custom-call | tf_op jit(solution)/shard_map/fused/pallas_call | solution.py:825
  152.6 2.5 %settle.1 = (bf16[384,512]{1,0:T(8,128)(2,1)}, bf16[1024,512]{1,0:T(8,128)(2,1)}, f32[32,256]{1,0:T(8,128)}) custom-call(bf16[384,512]{1,0:T(8,128)(2,1)} %get-tuple-element.9.refs_0_, bf16[1024,512]{1,0:T(8,128)(2,1)} %get-tuple-element.10.refs_1_, f32[32,256]{1,0:T(8,128)} %get-tuple-element.11.refs_2_), custom_call_target="tpu_custom_call" | custom-call | tf_op jit(solution)/shard_map/settle/pallas_call | solution.py:36

commit v2 on v1

--- a/solution.py
+++ b/solution.py
@@ -113,9 +113,6 @@
         states=((heads_n, mix_dim, mix_dim), F32),
         key_low=((rows_n, head), BF16),
         query_low=((tok_n, head), BF16),
-        query_grad=((tok_n, head), BF16),
-        gate_grad=((tok_n, 1), F32),
-        gw=((1, model), F32),
         kvr=((keys, 2 * head), BF16),
         e_buf=((ZN, keys, tok_n), F32),
         g_buf=((keys, tok_n), F32),
@@ -123,8 +120,8 @@
         pg=((keys, tok_n), BF16),
         zt=((ZN, 2, tok_n), F32),
         zt_r=((ZN, ZN, 2, tok_n), F32),
-        terms=((YN, CN, ZN, BLOCK, 2 * head), BF16),
-        term_r=((YN, ZN, BLOCK, 2 * head), BF16),
+        terms=((CN, ZN, YN, BLOCK, 2 * head), BF16),
+        term_r=((ZN, YN, BLOCK, 2 * head), BF16),
         qg=((ZN, tok_n, head), BF16),
         z_s=((2, ZN // 2, tok_n, head), BF16),
         z_r=((2, ZN // 2, tok_n, head), BF16),
@@ -133,15 +130,12 @@
         yd_s=((2, chunks, ROW, 2 * head), BF16),
         yd_r=((2, chunks, ROW, 2 * head), BF16),
         key_grad=((rows_n, head), BF16),
-        value_grad=((rows_n, head), BF16),
-        xf_s=((2, half, ROW, width), BF16),
-        xf_r=((2, half, ROW, width), BF16),
-        xd_s=((2, chunks, ROW, width), BF16),
-        xd_r=((2, chunks, ROW, width), BF16),
-        tf_s=((2, tok_n // 2, width), BF16),
-        tf_r=((2, tok_n // 2, width), BF16),
-        td_s=((2, 2, tok_n // 2, width), BF16),
-        td_r=((2, 2, tok_n // 2, width), BF16),
+        kgv=((XN, rows_n, 2 * head), BF16),
+        qga=((XN, tok_n, head), BF16),
+        gga=((XN, 8, tok_n), F32),
+        w_all=((XN, CN, 3, width // CN, head), BF16),
+        gwb=((8, model), F32),
+        gw_all=((XN, 8, width), F32),
         wbuf=((CN, YN, ZN, part, head), BF16),
         wc_r=((YN, ZN, part, head), BF16),
         w1=((YN, ZN, part, head), BF16),
@@ -154,19 +148,21 @@
         idsem=(2, CN, ZN),
         tokx=(2, 2, 2),
         cotz=(2, ZN // 2, 2),
-        qz=(2, ZN // 2, 2),
+        qz=(2, ZN // 2, 2, 2),
         gz=(2, ZN // 2, 2),
         kvy=(2, 2, 2, 4),
         kvd=(2, YN, 4),
-        zts=(2, ZN),
-        ters=(2, YN),
+        zts=(2, ZN, ZN),
+        ters=(2, ZN),
         zrs=(2, 2, ZN // 2),
         yfs=(2, 2, half),
         yds=(2, 2, chunks),
-        xfs=(2, 2, half),
-        xds=(2, 2, chunks),
-        tfs=(2, 2),
-        tds=(2, 2, 2),
+        xrs=(2, 2, 2, chunks),
+        tgs=(2, 2, 2),
+        ggs=(2, 2, 2),
+        wxs=(2, 3, XN),
+        wxd=(2, XN),
+        gws=(2, XN),
         wcs=(2,),
         wys=(2, YN),
         wzs=(2, ZN),
@@ -188,10 +184,9 @@
     tab_v, tab_s, code = get("tab_v", "tab_s", "code")
     kvr, e_buf, g_buf, sg, pg, zt, zt_r = get("kvr", "e_buf", "g_buf", "sg", "pg", "zt", "zt_r")
     terms, term_r, qg, z_s, z_r = get("terms", "term_r", "qg", "z_s", "z_r")
-    key_low, key_grad, value_grad = get("key_low", "key_grad", "value_grad")
-    query_low, query_grad, gate_grad = get("query_low", "query_grad", "gate_grad")
+    key_low, key_grad, query_low = get("key_low", "key_grad", "query_low")
+    kgv, qga, gga, w_all, gwb, gw_all = get("kgv", "qga", "gga", "w_all", "gwb", "gw_all")
     turned, mixed, states = get("turned", "mixed", "states")
-    gw = r["gw"]
 
     rows_n, model = rows_v.shape
     head = kw.shape[1]
@@ -270,7 +265,7 @@
 
     barrier = pltpu.get_barrier_semaphore()
     greeted = 0
-    for target in x_to:
+    for target in xs[1:]:
         pl.semaphore_signal(barrier, inc=1, device_id={"tp": target}, device_id_type=MESH)
         greeted += 1
     friends = [partner] + [at(z, ys[d], c) for d in range(1, YN)]
@@ -290,13 +285,13 @@
             ref = qc.at[source, 1, half_rows[d]]
         return remote(ref, ref, "cotz", (hop - 1, d), st_id=z_to[d])
 
-    def q_copies(hop, d):
+    def q_copies(hop, d, h):
         source = zs[(1 - hop) % ZN] if d == 0 else zs[(hop - 1) % ZN]
-        ref = qc.at[source, 0]
-        if hop == ZN // 2:
-            ref = qc.at[source, 0, half_rows[d]]
-        copies = [remote(ref, ref, "qz", (hop - 1, d), st_id=z_to[d])]
-        if hop < ZN // 2 or d == 0:
+        if hop == ZN // 2 and h != d:
+            return []
+        ref = qc.at[source, 0, half_rows[h]]
+        copies = [remote(ref, ref, "qz", (hop - 1, d, h), st_id=z_to[d])]
+        if h == d and (hop < ZN // 2 or d == 0):
             copies.append(
                 remote(gates.at[source], gates.at[source], "gz", (hop - 1, d), st_id=z_to[d])
             )
@@ -309,22 +304,21 @@
             ref = tok4.at[xs[XN - 1] if d == 0 else xs[1], half_rows[d]]
         return remote(ref, ref, "tokx", (hop - 1, d), tp_id=x_to[d])
 
+    def ids_copy(dc, dz):
+        return remote(
+            ids, r["ids_all"].at[c, z], "idsem", (dc, dz), st_id=at(zs[dz], y, other if dc else c)
+        )
+
+    id_peers = [(dc, dz) for dz in range(ZN) for dc in range(CN) if (dc, dz) != (0, 0)]
+    for dc, dz in id_peers:
+        go(ids_copy(dc, dz))
+    r["ids_all"][c, z] = ids[...]
     loads["tok"].wait()
     for d in range(2):
         go(tok_copy(1, d))
     loads["cot"].wait()
     for d in range(2):
         go(cot_copy(1, d))
-
-    def ids_copy(dc, dz):
-        return remote(
-            ids, r["ids_all"].at[c, z], "idsem", (dc, dz), st_id=at(zs[dz], y, other if dc else c)
-        )
-
-    id_peers = [(dc, dz) for dz in range(ZN) for dc in range(CN) if (dc, dz) != (0, 0)]
-    for dc, dz in id_peers:
-        go(ids_copy(dc, dz))
-    r["ids_all"][c, z] = ids[...]
 
     per_chunk = proj_rows // BLOCK
 
@@ -361,6 +355,115 @@
             go(kv_copy(1, d, k))
         go(kv_across(0, k))
 
+    gwb[...] = jnp.broadcast_to(gate_w[...].astype(F32), gwb.shape)
+    turned[...] = jnp.transpose(
+        jnp.concatenate(
+            [beta[...], decay[...], jnp.zeros((8 - 2 * heads_n, tok_n), F32)], axis=0
+        )
+    )
+    states[...] = jnp.zeros_like(states)
+    for key in ("mq", "mk", "mv", "qw"):
+        loads[key].wait()
+
+    def mix(b):
+        here = pl.ds(pl.multiple_of(b * SPAN, SPAN), SPAN)
+        for m in range(heads_n):
+            cols = pl.ds(m * mix_dim, mix_dim)
+            raw = turned[here, heads_n + m : heads_n + m + 1]
+            softplus = jnp.maximum(raw, 0.0) + jnp.log1p(jnp.exp(-jnp.abs(raw)))
+            mixed[here, cols], states[m] = mixer_span(
+                r["mq"][here, cols].astype(F32),
+                r["mk"][here, cols].astype(F32),
+                r["mv"][here, cols].astype(F32),
+                jax.nn.sigmoid(turned[here, m : m + 1]),
+                -rate[m] * softplus,
+                states[m],
+            )
+
+    spans_n = tok_n // SPAN
+
+    def cot_pass(hop):
+        for d in range(2):
+            cot_copy(hop - 1, d).wait_recv()
+            go(cot_copy(hop, d))
+
+    def q_pass(hop, first):
+        for d in range(2):
+            h = d if first else 1 - d
+            for copy in q_copies(hop - 1, d, h):
+                copy.wait_recv()
+            for copy in q_copies(hop, d, h):
+                go(copy)
+
+    def kv_pass(k):
+        for d, rel in ((0, YN - 1), (1, 1)):
+            kv_copy(1, d, k).wait_recv()
+            if (k < 2) == (d == 0):
+                go(kv_copy(2, d, k))
+            go(kv_across(rel, k))
+
+    w_half = width // CN
+
+    def w_copy(w, d):
+        rows = pl.ds(pl.multiple_of(xs[d] * width + c * w_half, w_half), w_half)
+        return remote(
+            (kw, vw, qw)[w].at[rows, :], w_all.at[x, c, w], "wxs", (w, d), tp_id=xs[d]
+        )
+
+    def w_across(d):
+        ref = w_all.at[xs[XN - d], c]
+        return remote(ref, ref, "wxd", (d,), st_id=partner)
+
+    def gw_copy(d):
+        cols = pl.ds(pl.multiple_of(xs[d] * width, width), width)
+        return remote(gwb.at[:, cols], gw_all.at[x], "gws", (d,), tp_id=xs[d])
+
+    pl.loop(0, 1)(mix)
+    cot_pass(2)
+    pl.loop(1, 2)(mix)
+    for d in range(2):
+        tok_copy(1, d).wait_recv()
+        go(tok_copy(2, d))
+    for d in range(1, XN):
+        for w in range(3):
+            go(w_copy(w, d))
+        go(gw_copy(d))
+    for w, ref in enumerate((kw, vw, qw)):
+        for h in range(CN):
+            w_all[x, h, w] = ref[pl.ds(pl.multiple_of(x * width + h * w_half, w_half), w_half), :]
+    gw_all[x] = gwb[:, pl.ds(pl.multiple_of(x * width, width), width)]
+    pl.loop(2, 3)(mix)
+    cot_pass(3)
+    kv_pass(0)
+    for d in range(2):
+        tok_copy(2, d).wait_recv()
+
+    gate_rows = jnp.broadcast_to(gate_w[...], (16, model))
+    logit = low_dot(gate_rows[:, :width], tok4[0], CONTRACT_LAST)
+    for i in range(1, XN):
+        logit += low_dot(gate_rows[:, i * width : (i + 1) * width], tok4[i], CONTRACT_LAST)
+    gates[z] = jax.nn.sigmoid(logit[:8])
+
+    @pl.loop(0, tok_n // ROW)
+    def _(k):
+        here = pl.ds(pl.multiple_of(k * ROW, ROW), ROW)
+        low = low_dot(tok4[0, here, :], qw[pl.ds(0, width), :])
+        for i in range(1, XN):
+            low += low_dot(tok4[i, here, :], qw[pl.ds(i * width, width), :])
+        low = low.astype(BF16)
+        query_low[here, :] = low
+        low = low.astype(F32)
+        scale = lax.rsqrt(jnp.mean(low * low, axis=-1, keepdims=True) + NORM_FLOOR)
+        qc[z, 0, here, :] = (low * scale).astype(BF16)
+
+    for h in range(2):
+        for d in range(2):
+            for copy in q_copies(1, d, d if h == 0 else 1 - d):
+                go(copy)
+    pl.loop(3, 4)(mix)
+    kv_pass(2)
+    cot_pass(4)
+    q_pass(2, True)
     for dc, dz in id_peers:
         ids_copy(dc, dz).wait_recv()
     every = jnp.concatenate(
@@ -383,94 +486,16 @@
     tab_v[1] = blk_tab
     tab_copy = pltpu.make_async_copy(tab_v, tab_s, r["load"].at[len(loads)])
     tab_copy.start()
-
-    gw[...] = gate_w[...].astype(F32)
-    turned[...] = jnp.transpose(
-        jnp.concatenate(
-            [beta[...], decay[...], jnp.zeros((8 - 2 * heads_n, tok_n), F32)], axis=0
-        )
-    )
-    states[...] = jnp.zeros_like(states)
-    for key in ("mq", "mk", "mv", "qw"):
-        loads[key].wait()
-
-    def mix(b):
-        here = pl.ds(pl.multiple_of(b * SPAN, SPAN), SPAN)
-        for m in range(heads_n):
-            cols = pl.ds(m * mix_dim, mix_dim)
-            raw = turned[here, heads_n + m : heads_n + m + 1]
-            softplus = jnp.maximum(raw, 0.0) + jnp.log1p(jnp.exp(-jnp.abs(raw)))
-            mixed[here, cols], states[m] = mixer_span(
-                r["mq"][here, cols].astype(F32),
-                r["mk"][here, cols].astype(F32),
-                r["mv"][here, cols].astype(F32),
-                jax.nn.sigmoid(turned[here, m : m + 1]),
-                -rate[m] * softplus,
-                states[m],
-            )
-
-    spans_n = tok_n // SPAN
-
-    def cot_pass(hop):
-        for d in range(2):
-            cot_copy(hop - 1, d).wait_recv()
-            go(cot_copy(hop, d))
-
-    def q_pass(hop):
-        for d in range(2):
-            for copy in q_copies(hop - 1, d):
-                copy.wait_recv()
-            for copy in q_copies(hop, d):
-                go(copy)
-
-    def kv_pass(k):
-        for d, rel in ((0, YN - 1), (1, 1)):
-            kv_copy(1, d, k).wait_recv()
-            if (k < 2) == (d == 0):
-                go(kv_copy(2, d, k))
-            go(kv_across(rel, k))
-
-    pl.loop(0, 1)(mix)
-    cot_pass(2)
-    for d in range(2):
-        tok_copy(1, d).wait_recv()
-        go(tok_copy(2, d))
-    pl.loop(1, 2)(mix)
-    for d in range(2):
-        tok_copy(2, d).wait_recv()
-
-    gate_rows = jnp.broadcast_to(gate_w[...], (16, model))
-    logit = low_dot(gate_rows[:, :width], tok4[0], CONTRACT_LAST)
-    for i in range(1, XN):
-        logit += low_dot(gate_rows[:, i * width : (i + 1) * width], tok4[i], CONTRACT_LAST)
-    gates[z] = jax.nn.sigmoid(logit[:8])
-
-    @pl.loop(0, tok_n // ROW)
-    def _(k):
-        here = pl.ds(pl.multiple_of(k * ROW, ROW), ROW)
-        low = low_dot(tok4[0, here, :], qw[pl.ds(0, width), :])
-        for i in range(1, XN):
-            low += low_dot(tok4[i, here, :], qw[pl.ds(i * width, width), :])
-        low = low.astype(BF16)
-        query_low[here, :] = low
-        low = low.astype(F32)
-        scale = lax.rsqrt(jnp.mean(low * low, axis=-1, keepdims=True) + NORM_FLOOR)
-        qc[z, 0, here, :] = (low * scale).astype(BF16)
-
-    for d in range(2):
-        for copy in q_copies(1, d):
-            go(copy)
-    cot_pass(3)
-    kv_pass(0)
-    pl.loop(2, 4)(mix)
-    kv_pass(2)
-    cot_pass(4)
-    q_pass(2)
-    pl.loop(4, spans_n)(mix)
+    q_pass(2, False)
     kv_pass(1)
-    q_pass(3)
+    q_pass(3, True)
     kv_pass(3)
-    q_pass(4)
+    q_pass(3, False)
+    for d in range(1, XN):
+        for w in range(3):
+            w_copy(w, d).wait_recv()
+        go(w_across(d))
+    q_pass(4, True)
     tab_copy.wait()
     lane_of = lax.broadcasted_iota(jnp.int32, (8, ZN * BLOCK), 1)
     for yi in range(YN):
@@ -487,7 +512,7 @@
             code[yi, which] = start + (lane_of & (BLOCK - 1))
     for d in range(2):
         cot_copy(ZN // 2, d).wait_recv()
-        for copy in q_copies(ZN // 2, d):
+        for copy in q_copies(ZN // 2 - 1, d, 1 - d) + q_copies(ZN // 2, d, d):
             copy.wait_recv()
     for d, k in ((0, 0), (1, 2), (0, 1), (1, 3)):
         kv_copy(2, d, k).wait_recv()
@@ -503,6 +528,11 @@
         for o in range(slab):
             local_at = jnp.clip(tab_s[0, c * ZN + reader, o], 0, passes - 1)
             kvr[pl.ds(o * BLOCK, BLOCK), :] = kv[o * passes + local_at]
+
+    def zt_copy(d, reader):
+        return remote(
+            zt.at[reader], zt_r.at[d, reader], "zts", (d, reader), st_id=at(zs[d], y, c)
+        )
 
     @pl.loop(0, ZN)
     def _(reader):
@@ -521,14 +551,8 @@
             product += jnp.sum(e * g_buf[here, :], axis=0, keepdims=True)
         zt[reader, 0:1, :] = total
         zt[reader, 1:2, :] = product * gates[reader, 0:1, :]
-
-    def zt_copy(d):
-        return remote(zt, zt_r.at[d], "zts", (d,), st_id=at(zs[d], y, c))
-
-    for d in range(1, ZN):
-        go(zt_copy(d))
-    for d in range(1, ZN):
-        zt_copy(d).wait_recv()
+        for d in (4, 3, 5, 2, 6, 1, 7):
+            zt_copy(d, reader).start()
 
     def summed(reader):
         both = zt[reader]
@@ -536,9 +560,15 @@
             both += zt_r[d, reader]
         return both[0:1, :], both[1:2, :]
 
+    def term_copy(reader):
+        return remote(
+            terms.at[other, reader], term_r.at[reader], "ters", (reader,), st_id=partner
+        )
+
     @pl.loop(0, ZN)
-    def _(i):
-        reader = lax.rem(z + jnp.where(lax.rem(i, 2) == 1, 4 - (i + 1) // 2, 4 + i // 2), ZN)
+    def _(reader):
+        for d in range(1, ZN):
+            zt_copy(d, reader).wait_recv()
         total, product = summed(reader)
         inverse = 1.0 / total
         mean = product * inverse
@@ -557,8 +587,9 @@
             for k in range(2 * ROW // BLOCK):
                 o = n * (2 * ROW // BLOCK) + k
                 piece = slice(k * BLOCK, (k + 1) * BLOCK)
-                terms[o // CN, o % CN, reader, :, :head] = key_term[piece]
-                terms[o // CN, o % CN, reader, :, head:] = value_term[piece]
+                terms[o % CN, reader, o // CN, :, :head] = key_term[piece]
+                terms[o % CN, reader, o // CN, :, head:] = value_term[piece]
+        term_copy(reader).start()
         qg[reader] = (low_dot(sg[...], kvr[:, :head], CONTRACT_FIRST) * score_scale).astype(BF16)
 
     def z_copy(hop, d):
@@ -587,13 +618,6 @@
                 ).astype(BF16)
             go(z_copy(hop, d))
 
-    def term_copy(rel):
-        return remote(
-            terms.at[ys[rel], other], term_r.at[ys[rel]], "ters", (rel,), st_id=partner
-        )
-
-    for rel in (2, 1, 3, 0):
-        go(term_copy(rel))
     for d in range(2):
         go(z_copy(1, d))
 
@@ -605,22 +629,18 @@
         ones = [
             jnp.where(rows == code[yi, which, 0:1, :], 1.0, 0.0).astype(BF16) for which in range(2)
         ]
-        return low_dot(ones[0], terms[yi, c].reshape(ZN * BLOCK, 2 * head)) + low_dot(
-            ones[1], term_r[yi].reshape(ZN * BLOCK, 2 * head)
+        return low_dot(ones[0], terms[c, :, yi].reshape(ZN * BLOCK, 2 * head)) + low_dot(
+            ones[1], term_r[:, yi].reshape(ZN * BLOCK, 2 * head)
         )
 
     yf_s, yf_r, yd_s, yd_r = get("yf_s", "yf_r", "yd_s", "yd_r")
-    xf_s, xf_r, xd_s, xd_r = get("xf_s", "xf_r", "xd_s", "xd_r")
-
-    def two_step(far_s, far_r, near_s, near_r, far_sem, near_sem, term, axis):
-        def target(d):
-            return {"st_id": y_to[d]} if axis == "y" else {"tp_id": x_to[d]}
-
+
+    def two_step(far_s, far_r, near_s, near_r, far_sem, near_sem, term):
         def far(d, j):
-            return remote(far_s.at[d, j], far_r.at[d, j], far_sem, (d, j), **target(d))
+            return remote(far_s.at[d, j], far_r.at[d, j], far_sem, (d, j), st_id=y_to[d])
 
         def near(d, q):
-            return remote(near_s.at[d, q], near_r.at[d, q], near_sem, (d, q), **target(d))
+            return remote(near_s.at[d, q], near_r.at[d, q], near_sem, (d, q), st_id=y_to[d])
 
         def send(j):
             for d in range(2):
@@ -648,16 +668,26 @@
 
         return send, forward, final
 
-    y_send, y_forward, y_final = two_step(yf_s, yf_r, yd_s, yd_r, "yfs", "yds", pick, "y")
-
-    def row_term(rel, q):
-        here = pl.ds(q * ROW, ROW)
-        cols = pl.ds(pl.multiple_of(xs[rel] * width, width), width)
-        return low_dot(key_grad[here, :], kw[cols, :], CONTRACT_LAST) + low_dot(
-            value_grad[here, :], vw[cols, :], CONTRACT_LAST
-        )
-
-    x_send, x_forward, x_final = two_step(xf_s, xf_r, xd_s, xd_r, "xfs", "xds", row_term, "x")
+    y_send, y_forward, y_final = two_step(yf_s, yf_r, yd_s, yd_r, "yfs", "yds", pick)
+
+    def x_copy(hop, d, q):
+        source = x if hop == 1 else (xs[XN - 1] if d == 0 else xs[1])
+        ref = kgv.at[source, pl.ds(q * ROW, ROW)]
+        return remote(ref, ref, "xrs", (hop - 1, d, q), tp_id=x_to[d])
+
+    def x_send(j):
+        for q in (j, j + half):
+            for d in range(2):
+                go(x_copy(1, d, q))
+
+    def x_forward(j):
+        for d in range(2):
+            q = j + half * d
+            x_copy(1, d, q).wait_recv()
+            go(x_copy(2, d, q))
+
+    def weight_of(head_at, w):
+        return w_all[head_at, :, w].reshape(width, head)
 
     def finish_rows(j):
         for q in (j, j + half):
@@ -666,41 +696,56 @@
             hat = value[:, :head]
             low = key_low[here, :].astype(F32)
             scale = lax.rsqrt(jnp.mean(low * low, axis=-1, keepdims=True) + NORM_FLOOR)
-            key_grad[here, :] = (
+            grad = (
                 scale * hat
                 - scale * scale * scale * low * jnp.mean(low * hat, axis=-1, keepdims=True)
             ).astype(BF16)
-            value_grad[here, :] = value[:, head:].astype(BF16)
+            key_grad[here, :] = grad
+            kgv[x, here, :head] = grad
+            kgv[x, here, head:] = value[:, head:].astype(BF16)
 
     def finish_out(j):
-        for q in (j, j + half):
-            out_ref[pl.ds(q * ROW, ROW), :] = x_final(q).astype(out_ref.dtype)
-
-    for rel in (2, 1, 3):
-        term_copy(rel).wait_recv()
+        for d in range(2):
+            q = j + half * d
+            here = pl.ds(q * ROW, ROW)
+            x_copy(1, 1 - d, q).wait_recv()
+            x_copy(2, d, q).wait_recv()
+            value = jnp.zeros((ROW, width), F32)
+            for i in range(XN):
+                value += low_dot(kgv[i, here, :head], weight_of(i, 0), CONTRACT_LAST)
+                value += low_dot(kgv[i, here, head:], weight_of(i, 1), CONTRACT_LAST)
+            out_ref[here, :] = value.astype(out_ref.dtype)
+
+    @pl.loop(0, ZN)
+    def _(reader):
+        term_copy(reader).wait_recv()
+
     y_send(0)
+    pl.loop(4, 5)(mix)
+    y_forward(0)
     y_send(1)
-    y_forward(0)
     z_pass(2)
-    y_send(2)
-    y_forward(1)
-    z_pass(3)
-    y_send(3)
-    term_copy(0).wait_recv()
+    pl.loop(5, spans_n)(mix)
     finish_rows(0)
     x_send(0)
+    z_pass(3)
+    y_forward(1)
+    y_send(2)
+    x_forward(0)
     z_pass(4)
+    finish_rows(1)
+    x_send(1)
     y_forward(2)
-    x_forward(0)
+    y_send(3)
 
     for d in range(2):
         z_copy(ZN // 2, d).wait_recv()
     total, product = summed(z)
-    stack = jnp.transpose(
-        jnp.concatenate(
-            [gates[z, 0:1, :], product / total, jnp.zeros((6, tok_n), F32)], axis=0
-        )
-    )
+    along = exact_dot(
+        jnp.ones((8, head), F32), qc[z, 1].astype(F32) * mixed[...], CONTRACT_LAST
+    )
+    opened = gates[z]
+    gga[x] = (1.0 - opened) * (product / total - opened * along)
 
     for k in range(tok_n // ROW):
         here = pl.ds(k * ROW, ROW)
@@ -709,52 +754,38 @@
             hat_grad += z_r[d, ZN // 2 - 1, here, :].astype(F32)
         low = query_low[here, :].astype(F32)
         scale = lax.rsqrt(jnp.mean(low * low, axis=-1, keepdims=True) + NORM_FLOOR)
-        query_grad[here, :] = (
+        qga[x, here, :] = (
             scale * hat_grad
             - scale * scale * scale * low * jnp.mean(low * hat_grad, axis=-1, keepdims=True)
         ).astype(BF16)
-        opened = stack[k * ROW : (k + 1) * ROW, 0:1]
-        ratio = stack[k * ROW : (k + 1) * ROW, 1:2]
-        along = jnp.sum(
-            qc[z, 1, here, :].astype(F32) * mixed[here, :], axis=-1, keepdims=True
-        )
-        gate_grad[here, :] = (1.0 - opened) * (ratio - opened * along)
-
-    tf_s, tf_r, td_s, td_r = get("tf_s", "tf_r", "td_s", "td_r")
-
-    def token_term(rel, h):
-        cols = pl.ds(pl.multiple_of(xs[rel] * width, width), width)
-        here = half_rows[h]
-        return (
-            low_dot(query_grad[here, :], qw[cols, :], CONTRACT_LAST)
-            + gate_grad[here, :] * gw[:, cols]
-        )
-
-    def t_far(d):
-        return remote(tf_s.at[d], tf_r.at[d], "tfs", (d,), tp_id=x_to[d])
-
-    def t_near(d, h):
-        return remote(td_s.at[d, h], td_r.at[d, h], "tds", (d, h), tp_id=x_to[d])
+
+    def t_copies(hop, d):
+        source = x if hop == 1 else (xs[XN - 1] if d == 0 else xs[1])
+        ref = qga.at[source] if hop == 1 else qga.at[source, half_rows[d]]
+        copies = [remote(ref, ref, "tgs", (hop - 1, d), tp_id=x_to[d])]
+        if hop == 1 or d == 0:
+            copies.append(
+                remote(gga.at[source], gga.at[source], "ggs", (hop - 1, d), tp_id=x_to[d])
+            )
+        return copies
 
     for d in range(2):
-        tf_s[d] = token_term(2, d).astype(BF16)
-        go(t_far(d))
-    for d in range(2):
-        td_s[d, 1 - d] = token_term(1 if d == 0 else 3, 1 - d).astype(BF16)
-        go(t_near(d, 1 - d))
-
-    finish_rows(1)
-    x_send(1)
+        for copy in t_copies(1, d):
+            go(copy)
+    x_forward(1)
+    finish_rows(2)
+    x_send(2)
     y_forward(3)
     for d in range(2):
-        value = token_term(1 if d == 0 else 3, d)
-        t_far(d).wait_recv()
-        td_s[d, d] = (value + tf_r[d].astype(F32)).astype(BF16)
-        go(t_near(d, d))
-    x_forward(1)
+        for copy in t_copies(1, d):
+            copy.wait_recv()
+        for copy in t_copies(2, d):
+            go(copy)
+    for d in range(1, XN):
+        w_across(d).wait_recv()
+        gw_copy(d).wait_recv()
     finish_out(0)
-    finish_rows(2)
-    x_send(2)
+    x_forward(2)
     finish_rows(3)
     x_send(3)
 
@@ -770,7 +801,7 @@
 
     wc_copy = remote(wbuf.at[other], wc_r, "wcs", (), st_id=partner)
     go(wc_copy)
-    x_forward(2)
+    finish_out(1)
     wc_copy.wait_recv()
     for yi in range(YN):
         w1[yi] = (wbuf[c, yi].astype(F32) + wc_r[yi].astype(F32)).astype(BF16)
@@ -783,7 +814,7 @@
 
     for d in (2, 1, 3):
         go(wy_copy(d))
-    finish_out(1)
+    x_forward(3)
     for d in range(1, YN):
         wy_copy(d).wait_recv()
     gathered = w1[y].astype(F32)
@@ -792,15 +823,18 @@
     w2[...] = gathered.astype(BF16)
     for d in (4, 3, 5, 2, 6, 1, 7):
         go(wz_copy(d))
-    x_forward(3)
-    for h in range(2):
-        value = token_term(0, h)
-        for d in range(2):
-            t_near(d, h).wait_recv()
-        tok_out[half_rows[h], :] = (
-            value + td_r[0, h].astype(F32) + td_r[1, h].astype(F32)
-        ).astype(tok_out.dtype)
     finish_out(2)
+    for d in range(2):
+        for copy in t_copies(2, d):
+            copy.wait_recv()
+    gate_rows = jnp.concatenate([gga[i, 0:1, :] for i in range(XN)] + [jnp.zeros((4, tok_n), F32)])
+    gate_cols = jnp.concatenate([gw_all[i, 0:1, :] for i in range(XN)] + [jnp.zeros((4, width), F32)])
+    for k in range(tok_n // ROW):
+        here = pl.ds(k * ROW, ROW)
+        value = exact_dot(gate_rows[:, k * ROW : (k + 1) * ROW], gate_cols, CONTRACT_FIRST)
+        for i in range(XN):
+            value += low_dot(qga[i, here, :], weight_of(i, 2), CONTRACT_LAST)
+        tok_out[here, :] = value.astype(tok_out.dtype)
     for d in range(1, ZN):
         wz_copy(d).wait_recv()
     weight = w2[z].astype(F32)
@@ -810,6 +844,12 @@
     finish_out(3)
     for copy in started:
         copy.wait_send()
+
+    @pl.loop(0, ZN)
+    def _(reader):
+        term_copy(reader).wait_send()
+        for d in range(1, ZN):
+            zt_copy(d, reader).wait_send()
 
 
 def fused_call(rate, ids, gate_w, beta, decay, tok, cot, mq, mk, mv, qw, kw, vw, rows):

time: 156 us -> 148 us (0.949)
  Pallas kernels: 153 us -> 146 us
    pallas_call x1, Pallas kernels: 151 us -> 144 us  [fused_call(): pl.pallas_call(functools.partial(fused_kernel, names), out_shape=(jax.Sha...]
where the time goes in v2:
time: 148 us
  Pallas kernels  146 us (99%)
    pallas_call x1, Pallas kernels, fused_call(): pl.pallas_call(functools.partial(fused_kernel, names), out_shape=(jax.Sha...  144 us

profile of v2, /device:TPU:1, one launch (start us, length us, event | category | flops | bytes accessed | tf_op | source)
XLA Modules:
  0.0 148.2 jit_solution(15957850425855498557)
XLA Ops:
  0.6 0.8 copy.18
  1.4 0.1 reshape.15
  1.5 0.6 pad.4.refs_1_
  2.1 143.6 %fused.1 = (bf16[384,512]{1,0:T(8,128)(2,1)}, bf16[1024,512]{1,0:T(8,128)(2,1)}, f32[32,256]{1,0:T(8,128)}) custom-call(f32[2]{0:T(128)} %refs_0_.1, s32[8,128]{1,0:T(8,128)} %pad.4.refs_1_, bf16[1,2048]{1,0:T(2,128)(2,1)} %refs_2_.1, f32[2,384]{1,0:T(2,128)} %refs_3_.1, f32[2,384]{1,0:T(2,128)} %refs_4_.1, bf16[384,512]{1,0:T(8,128)(2,1)} %refs_5_.1, ...), custom_call_target="tpu_custom_call" | custom-call | tf_op jit(solution)/shard_map/fused/pallas_call | solution.py:865
  145.7 2.5 %settle.1 = (bf16[384,512]{1,0:T(8,128)(2,1)}, bf16[1024,512]{1,0:T(8,128)(2,1)}, f32[32,256]{1,0:T(8,128)}) custom-call(bf16[384,512]{1,0:T(8,128)(2,1)} %get-tuple-element.9.refs_0_, bf16[1024,512]{1,0:T(8,128)(2,1)} %get-tuple-element.10.refs_1_, f32[32,256]{1,0:T(8,128)} %get-tuple-element.11.refs_2_), custom_call_target="tpu_custom_call" | custom-call | tf_op jit(solution)/shard_map/settle/pallas_call | solution.py:36

commit v3 on v2

--- a/solution.py
+++ b/solution.py
@@ -146,7 +146,7 @@
     sems = dict(
         load=(16,),
         idsem=(2, CN, ZN),
-        tokx=(2, 2, 2),
+        tokx=(2, 2, 2, 2),
         cotz=(2, ZN // 2, 2),
         qz=(2, ZN // 2, 2, 2),
         gz=(2, ZN // 2, 2),
@@ -297,12 +297,10 @@
             )
         return copies
 
-    def tok_copy(hop, d):
-        if hop == 1:
-            ref = tok4.at[x]
-        else:
-            ref = tok4.at[xs[XN - 1] if d == 0 else xs[1], half_rows[d]]
-        return remote(ref, ref, "tokx", (hop - 1, d), tp_id=x_to[d])
+    def tok_copy(hop, d, h):
+        source = x if hop == 1 else (xs[XN - 1] if d == 0 else xs[1])
+        ref = tok4.at[source, half_rows[h]]
+        return remote(ref, ref, "tokx", (hop - 1, d, h), tp_id=x_to[d])
 
     def ids_copy(dc, dz):
         return remote(
@@ -315,7 +313,9 @@
     r["ids_all"][c, z] = ids[...]
     loads["tok"].wait()
     for d in range(2):
-        go(tok_copy(1, d))
+        go(tok_copy(1, d, d))
+    for d in range(2):
+        go(tok_copy(1, d, 1 - d))
     loads["cot"].wait()
     for d in range(2):
         go(cot_copy(1, d))
@@ -420,23 +420,15 @@
 
     pl.loop(0, 1)(mix)
     cot_pass(2)
-    pl.loop(1, 2)(mix)
-    for d in range(2):
-        tok_copy(1, d).wait_recv()
-        go(tok_copy(2, d))
-    for d in range(1, XN):
-        for w in range(3):
-            go(w_copy(w, d))
-        go(gw_copy(d))
-    for w, ref in enumerate((kw, vw, qw)):
-        for h in range(CN):
-            w_all[x, h, w] = ref[pl.ds(pl.multiple_of(x * width + h * w_half, w_half), w_half), :]
-    gw_all[x] = gwb[:, pl.ds(pl.multiple_of(x * width, width), width)]
-    pl.loop(2, 3)(mix)
+    for d in range(2):
+        tok_copy(1, d, d).wait_recv()
+        go(tok_copy(2, d, d))
+    pl.loop(1, 3)(mix)
     cot_pass(3)
     kv_pass(0)
     for d in range(2):
-        tok_copy(2, d).wait_recv()
+        tok_copy(1, d, 1 - d).wait_recv()
+        tok_copy(2, d, d).wait_recv()
 
     gate_rows = jnp.broadcast_to(gate_w[...], (16, model))
     logit = low_dot(gate_rows[:, :width], tok4[0], CONTRACT_LAST)
@@ -460,10 +452,19 @@
         for d in range(2):
             for copy in q_copies(1, d, d if h == 0 else 1 - d):
                 go(copy)
+    for d in range(1, XN):
+        for w in range(3):
+            go(w_copy(w, d))
+        go(gw_copy(d))
+    for w, ref in enumerate((kw, vw, qw)):
+        for h in range(CN):
+            w_all[x, h, w] = ref[pl.ds(pl.multiple_of(x * width + h * w_half, w_half), w_half), :]
+    gw_all[x] = gwb[:, pl.ds(pl.multiple_of(x * width, width), width)]
     pl.loop(3, 4)(mix)
     kv_pass(2)
+    q_pass(2, True)
+    kv_pass(1)
     cot_pass(4)
-    q_pass(2, True)
     for dc, dz in id_peers:
         ids_copy(dc, dz).wait_recv()
     every = jnp.concatenate(
@@ -487,15 +488,11 @@
     tab_copy = pltpu.make_async_copy(tab_v, tab_s, r["load"].at[len(loads)])
     tab_copy.start()
     q_pass(2, False)
-    kv_pass(1)
+    kv_pass(3)
     q_pass(3, True)
-    kv_pass(3)
     q_pass(3, False)
-    for d in range(1, XN):
-        for w in range(3):
-            w_copy(w, d).wait_recv()
-        go(w_across(d))
     q_pass(4, True)
+    pl.loop(4, 5)(mix)
     tab_copy.wait()
     lane_of = lax.broadcasted_iota(jnp.int32, (8, ZN * BLOCK), 1)
     for yi in range(YN):
@@ -721,22 +718,29 @@
         term_copy(reader).wait_recv()
 
     y_send(0)
-    pl.loop(4, 5)(mix)
+    pl.loop(5, spans_n)(mix)
     y_forward(0)
     y_send(1)
     z_pass(2)
-    pl.loop(5, spans_n)(mix)
     finish_rows(0)
     x_send(0)
-    z_pass(3)
     y_forward(1)
     y_send(2)
+    z_pass(3)
+    for d in range(1, XN):
+        for w in range(3):
+            w_copy(w, d).wait_recv()
+        go(w_across(d))
+    finish_rows(1)
     x_forward(0)
+    x_send(1)
     z_pass(4)
-    finish_rows(1)
-    x_send(1)
     y_forward(2)
     y_send(3)
+    finish_rows(2)
+    x_send(2)
+    x_forward(1)
+    y_forward(3)
 
     for d in range(2):
         z_copy(ZN // 2, d).wait_recv()
@@ -772,10 +776,22 @@
     for d in range(2):
         for copy in t_copies(1, d):
             go(copy)
-    x_forward(1)
-    finish_rows(2)
-    x_send(2)
-    y_forward(3)
+    finish_rows(3)
+    x_send(3)
+    x_forward(2)
+
+    wbuf, wc_r, w1, wy_r, w2, wz_r = get("wbuf", "wc_r", "w1", "wy_r", "w2", "wz_r")
+    part = weight_ref.shape[0]
+
+    @pl.loop(0, ZN)
+    def _(k):
+        cols = pl.ds(pl.multiple_of(k * slab * part, slab * part), slab * part)
+        tile = low_dot(rows_v[:, cols], key_grad[...], CONTRACT_FIRST).astype(BF16)
+        for o in range(slab):
+            wbuf[o % CN, o // CN, k] = tile[o * part : (o + 1) * part]
+
+    wc_copy = remote(wbuf.at[other], wc_r, "wcs", (), st_id=partner)
+    go(wc_copy)
     for d in range(2):
         for copy in t_copies(1, d):
             copy.wait_recv()
@@ -785,23 +801,6 @@
         w_across(d).wait_recv()
         gw_copy(d).wait_recv()
     finish_out(0)
-    x_forward(2)
-    finish_rows(3)
-    x_send(3)
-
-    wbuf, wc_r, w1, wy_r, w2, wz_r = get("wbuf", "wc_r", "w1", "wy_r", "w2", "wz_r")
-    part = weight_ref.shape[0]
-
-    @pl.loop(0, ZN)
-    def _(k):
-        cols = pl.ds(pl.multiple_of(k * slab * part, slab * part), slab * part)
-        tile = low_dot(rows_v[:, cols], key_grad[...], CONTRACT_FIRST).astype(BF16)
-        for o in range(slab):
-            wbuf[o % CN, o // CN, k] = tile[o * part : (o + 1) * part]
-
-    wc_copy = remote(wbuf.at[other], wc_r, "wcs", (), st_id=partner)
-    go(wc_copy)
-    finish_out(1)
     wc_copy.wait_recv()
     for yi in range(YN):
         w1[yi] = (wbuf[c, yi].astype(F32) + wc_r[yi].astype(F32)).astype(BF16)
@@ -814,6 +813,7 @@
 
     for d in (2, 1, 3):
         go(wy_copy(d))
+    finish_out(1)
     x_forward(3)
     for d in range(1, YN):
         wy_copy(d).wait_recv()

time: 148 us -> 137 us (0.926); the launches traced: 148 us -> 135 us
  Pallas kernels: 146 us -> 133 us
    pallas_call x1, Pallas kernels: 144 us -> 131 us  [fused_call(): pl.pallas_call(functools.partial(fused_kernel, names), out_shape=(jax.Sha...]
where the time goes in v3:
time: 137 us; the launch traced here: 135 us
  Pallas kernels  133 us (97%)
  local copies, waits for them, and re-layouts  1.45 us (1%)
    pallas_call x1, Pallas kernels, fused_call(): pl.pallas_call(functools.partial(fused_kernel, names), out_shape=(jax.Sha...  131 us

profile of v3, /device:TPU:1, one launch (start us, length us, event | category | flops | bytes accessed | tf_op | source)
XLA Modules:
  0.0 135.3 jit_solution(5923172982415171947)
XLA Ops:
  0.6 0.8 copy.18
  1.4 0.1 reshape.15
  1.5 0.6 pad.4.refs_1_
  2.1 130.8 %fused.1 = (bf16[384,512]{1,0:T(8,128)(2,1)}, bf16[1024,512]{1,0:T(8,128)(2,1)}, f32[32,256]{1,0:T(8,128)}) custom-call(f32[2]{0:T(128)} %refs_0_.1, s32[8,128]{1,0:T(8,128)} %pad.4.refs_1_, bf16[1,2048]{1,0:T(2,128)(2,1)} %refs_2_.1, f32[2,384]{1,0:T(2,128)} %refs_3_.1, f32[2,384]{1,0:T(2,128)} %refs_4_.1, bf16[384,512]{1,0:T(8,128)(2,1)} %refs_5_.1, ...), custom_call_target="tpu_custom_call" | custom-call | tf_op jit(solution)/shard_map/fused/pallas_call | solution.py:865
  132.9 2.5 %settle.1 = (bf16[384,512]{1,0:T(8,128)(2,1)}, bf16[1024,512]{1,0:T(8,128)(2,1)}, f32[32,256]{1,0:T(8,128)}) custom-call(bf16[384,512]{1,0:T(8,128)(2,1)} %get-tuple-element.9.refs_0_, bf16[1024,512]{1,0:T(8,128)(2,1)} %get-tuple-element.10.refs_1_, f32[32,256]{1,0:T(8,128)} %get-tuple-element.11.refs_2_), custom_call_target="tpu_custom_call" | custom-call | tf_op jit(solution)/shard_map/settle/pallas_call | solution.py:36

commit v4 on v3

--- a/solution.py
+++ b/solution.py
@@ -24,6 +24,8 @@
 
 ZN, YN, CN, XN = 8, 4, 2, 4
 ROW = 128
+SENDS = ("id0", "id1", "tokx", "cotz", "qz", "gz", "kvy", "kvd", "zts", "ters", "zrs", "yfs")
+SENDS += ("yds", "xrs", "tgs", "ggs", "wxs", "wxd", "gws", "wcs", "wys", "wzs")
 
 
 def settle_kernel(*refs):
@@ -142,30 +144,36 @@
         wy_r=((YN, ZN, part, head), BF16),
         w2=((ZN, part, head), BF16),
         wz_r=((ZN, part, head), BF16),
+        tok_v=((tok_n, width), BF16),
+        out_v=((rows_n, width), BF16),
+        weight_v=((part, head), F32),
+        w_acc=((model, head), F32),
     )
     sems = dict(
         load=(16,),
-        idsem=(2, CN, ZN),
-        tokx=(2, 2, 2, 2),
-        cotz=(2, ZN // 2, 2),
-        qz=(2, ZN // 2, 2, 2),
-        gz=(2, ZN // 2, 2),
-        kvy=(2, 2, 2, 4),
-        kvd=(2, YN, 4),
-        zts=(2, ZN, ZN),
-        ters=(2, ZN),
-        zrs=(2, 2, ZN // 2),
-        yfs=(2, 2, half),
-        yds=(2, 2, chunks),
-        xrs=(2, 2, 2, chunks),
-        tgs=(2, 2, 2),
-        ggs=(2, 2, 2),
-        wxs=(2, 3, XN),
-        wxd=(2, XN),
-        gws=(2, XN),
-        wcs=(2,),
-        wys=(2, YN),
-        wzs=(2, ZN),
+        outs=(3,),
+        send=(len(SENDS),),
+        idsem=(CN,),
+        tokx=(2, 2, 2),
+        cotz=(ZN // 2, 2),
+        qz=(ZN // 2, 2, 2),
+        gz=(ZN // 2, 2),
+        kvy=(2, 2, 4),
+        kvd=(1,),
+        zts=(ZN,),
+        ters=(1,),
+        zrs=(2, ZN // 2),
+        yfs=(2, half),
+        yds=(chunks,),
+        xrs=(2, chunks),
+        tgs=(2, 2),
+        ggs=(2, 2),
+        wxs=(1,),
+        wxd=(1,),
+        gws=(1,),
+        wcs=(1,),
+        wys=(1,),
+        wzs=(1,),
     )
     return vmem, sems
 
@@ -177,7 +185,7 @@
         return [r[k] for k in keys]
 
     rate, ids, gate_w, beta, decay = get("rate", "ids", "gate_w", "beta", "decay")
-    tok_out, out_ref, weight_ref = get("tok_out", "out_ref", "weight_ref")
+    tok_out, out_ref, weight_ref = get("tok_v", "out_v", "weight_v")
     rows_v, kw, vw, qw, tok4, kv, qc, gates = get(
         "rows_v", "kw", "vw", "qw", "tok4", "kv", "qc", "gates"
     )
@@ -221,10 +229,7 @@
     y_to = (at(z, ys[1], c), at(z, ys[YN - 1], c))
     z_to = (at(zs[1], y, c), at(zs[ZN - 1], y, c))
 
-    started = []
-
-    def remote(src, dst, sem, index, st_id=None, tp_id=None):
-        sems = r[sem]
+    def remote(src, dst, sem, index, st_id=None, tp_id=None, group=None):
         device = {}
         if st_id is not None:
             device["st"] = st_id
@@ -233,15 +238,20 @@
         return pltpu.make_async_remote_copy(
             src_ref=src,
             dst_ref=dst,
-            send_sem=sems.at[(0, *index)],
-            recv_sem=sems.at[(1, *index)],
+            send_sem=r["send"].at[SENDS.index(group or sem)],
+            recv_sem=r[sem].at[index],
             device_id=device,
             device_id_type=MESH,
         )
 
     def go(copy):
         copy.start()
-        started.append(copy)
+
+    def all_of(ref, sem, index, group=None):
+        return remote(ref, ref, sem, index, st_id=partner, group=group)
+
+    def leave(index, src, dst):
+        pltpu.make_async_copy(src, dst, r["outs"].at[index]).start()
 
     loads = {}
 
@@ -304,7 +314,12 @@
 
     def ids_copy(dc, dz):
         return remote(
-            ids, r["ids_all"].at[c, z], "idsem", (dc, dz), st_id=at(zs[dz], y, other if dc else c)
+            ids,
+            r["ids_all"].at[c, z],
+            "idsem",
+            (dc,),
+            st_id=at(zs[dz], y, other if dc else c),
+            group="id1" if dc else "id0",
         )
 
     id_peers = [(dc, dz) for dz in range(ZN) for dc in range(CN) if (dc, dz) != (0, 0)]
@@ -332,7 +347,7 @@
 
     def kv_across(rel, k):
         ref = kv_piece(ys[rel], c, k)
-        return remote(ref, ref, "kvd", (rel, k), st_id=partner)
+        return remote(ref, ref, "kvd", (0,), st_id=partner)
 
     loads["kw"].wait()
     loads["vw"].wait()
@@ -407,16 +422,16 @@
     def w_copy(w, d):
         rows = pl.ds(pl.multiple_of(xs[d] * width + c * w_half, w_half), w_half)
         return remote(
-            (kw, vw, qw)[w].at[rows, :], w_all.at[x, c, w], "wxs", (w, d), tp_id=xs[d]
+            (kw, vw, qw)[w].at[rows, :], w_all.at[x, c, w], "wxs", (0,), tp_id=xs[d]
         )
 
     def w_across(d):
         ref = w_all.at[xs[XN - d], c]
-        return remote(ref, ref, "wxd", (d,), st_id=partner)
+        return remote(ref, ref, "wxd", (0,), st_id=partner)
 
     def gw_copy(d):
         cols = pl.ds(pl.multiple_of(xs[d] * width, width), width)
-        return remote(gwb.at[:, cols], gw_all.at[x], "gws", (d,), tp_id=xs[d])
+        return remote(gwb.at[:, cols], gw_all.at[x], "gws", (0,), tp_id=xs[d])
 
     pl.loop(0, 1)(mix)
     cot_pass(2)
@@ -465,8 +480,9 @@
     q_pass(2, True)
     kv_pass(1)
     cot_pass(4)
-    for dc, dz in id_peers:
-        ids_copy(dc, dz).wait_recv()
+    id_refs = (r["ids_all"].at[0, pl.ds(0, ZN - 1)], r["ids_all"].at[1])
+    for dc in range(CN):
+        all_of(id_refs[dc], "idsem", (dc,), f"id{dc}").wait_recv()
     every = jnp.concatenate(
         [r["ids_all"][ci, zi, 0:1, :] for ci in range(CN) for zi in range(ZN)], axis=0
     )
@@ -514,9 +530,8 @@
     for d, k in ((0, 0), (1, 2), (0, 1), (1, 3)):
         kv_copy(2, d, k).wait_recv()
         go(kv_across(2, k))
-    for rel in range(YN):
-        for k in range(4):
-            kv_across(rel, k).wait_recv()
+    kv_across_all = all_of(kv.at[pl.ds(0, YN * passes)], "kvd", (0,))
+    kv_across_all.wait_recv()
 
     tok_block = lax.shift_right_logical(lax.broadcasted_iota(jnp.int32, (BLOCK, tok_n), 1), 6)
     key_halves = [pl.ds(i * ROW * 2, ROW * 2) for i in range(slab * BLOCK // (2 * ROW))]
@@ -528,7 +543,7 @@
 
     def zt_copy(d, reader):
         return remote(
-            zt.at[reader], zt_r.at[d, reader], "zts", (d, reader), st_id=at(zs[d], y, c)
+            zt.at[reader], zt_r.at[d, reader], "zts", (reader,), st_id=at(zs[d], y, c)
         )
 
     @pl.loop(0, ZN)
@@ -559,13 +574,12 @@
 
     def term_copy(reader):
         return remote(
-            terms.at[other, reader], term_r.at[reader], "ters", (reader,), st_id=partner
+            terms.at[other, reader], term_r.at[reader], "ters", (0,), st_id=partner
         )
 
     @pl.loop(0, ZN)
     def _(reader):
-        for d in range(1, ZN):
-            zt_copy(d, reader).wait_recv()
+        all_of(zt_r.at[pl.ds(1, ZN - 1), reader], "zts", (reader,)).wait_recv()
         total, product = summed(reader)
         inverse = 1.0 / total
         mean = product * inverse
@@ -637,7 +651,7 @@
             return remote(far_s.at[d, j], far_r.at[d, j], far_sem, (d, j), st_id=y_to[d])
 
         def near(d, q):
-            return remote(near_s.at[d, q], near_r.at[d, q], near_sem, (d, q), st_id=y_to[d])
+            return remote(near_s.at[d, q], near_r.at[d, q], near_sem, (q,), st_id=y_to[d])
 
         def send(j):
             for d in range(2):
@@ -659,8 +673,7 @@
 
         def final(q):
             value = term(0, q)
-            for d in range(2):
-                near(d, q).wait_recv()
+            all_of(near_r.at[:, q], near_sem, (q,)).wait_recv()
             return value + near_r[0, q].astype(F32) + near_r[1, q].astype(F32)
 
         return send, forward, final
@@ -670,7 +683,8 @@
     def x_copy(hop, d, q):
         source = x if hop == 1 else (xs[XN - 1] if d == 0 else xs[1])
         ref = kgv.at[source, pl.ds(q * ROW, ROW)]
-        return remote(ref, ref, "xrs", (hop - 1, d, q), tp_id=x_to[d])
+        passed_on = hop == 1 and (q < half) == (d == 0)
+        return remote(ref, ref, "xrs", (0 if passed_on else 1, q), tp_id=x_to[d])
 
     def x_send(j):
         for q in (j, j + half):
@@ -705,17 +719,37 @@
         for d in range(2):
             q = j + half * d
             here = pl.ds(q * ROW, ROW)
-            x_copy(1, 1 - d, q).wait_recv()
-            x_copy(2, d, q).wait_recv()
+            all_of(kgv.at[pl.ds(0, 2), here], "xrs", (1, q)).wait_recv()
             value = jnp.zeros((ROW, width), F32)
             for i in range(XN):
                 value += low_dot(kgv[i, here, :head], weight_of(i, 0), CONTRACT_LAST)
                 value += low_dot(kgv[i, here, head:], weight_of(i, 1), CONTRACT_LAST)
             out_ref[here, :] = value.astype(out_ref.dtype)
-
-    @pl.loop(0, ZN)
-    def _(reader):
-        term_copy(reader).wait_recv()
+            leave(0, out_ref.at[here, :], r["out_ref"].at[here, :])
+
+    wbuf, wc_r, w1, wy_r, w2, wz_r = get("wbuf", "wc_r", "w1", "wy_r", "w2", "wz_r")
+    w_acc = r["w_acc"]
+    part = weight_ref.shape[0]
+
+    def weight_rows(j):
+        low, high = pl.ds(j * ROW, ROW), pl.ds((j + half) * ROW, ROW)
+        grad = jnp.concatenate([key_grad[low, :], key_grad[high, :]], axis=0)
+
+        @pl.loop(0, ZN)
+        def _(k):
+            cols = pl.ds(pl.multiple_of(k * slab * part, slab * part), slab * part)
+            rows = jnp.concatenate([rows_v[low, cols], rows_v[high, cols]], axis=0)
+            tile = low_dot(rows, grad, CONTRACT_FIRST)
+            if j > 0:
+                tile += w_acc[cols, :]
+            if j < half - 1:
+                w_acc[cols, :] = tile
+            else:
+                tile = tile.astype(BF16)
+                for o in range(slab):
+                    wbuf[o % CN, o // CN, k] = tile[o * part : (o + 1) * part]
+
+    all_of(term_r, "ters", (0,)).wait_recv()
 
     y_send(0)
     pl.loop(5, spans_n)(mix)
@@ -727,19 +761,23 @@
     y_forward(1)
     y_send(2)
     z_pass(3)
+    all_of(w_all.at[pl.ds(0, XN - 1), 0], "wxs", (0,)).wait_recv()
     for d in range(1, XN):
-        for w in range(3):
-            w_copy(w, d).wait_recv()
         go(w_across(d))
+    weight_rows(0)
     finish_rows(1)
     x_forward(0)
     x_send(1)
     z_pass(4)
     y_forward(2)
     y_send(3)
+    weight_rows(1)
+    all_of(w_all.at[pl.ds(0, XN - 1), 0], "wxd", (0,)).wait_recv()
+    all_of(gw_all.at[pl.ds(0, XN - 1)], "gws", (0,)).wait_recv()
+    finish_out(0)
     finish_rows(2)
+    x_forward(1)
     x_send(2)
-    x_forward(1)
     y_forward(3)
 
     for d in range(2):
@@ -776,54 +814,41 @@
     for d in range(2):
         for copy in t_copies(1, d):
             go(copy)
+    weight_rows(2)
+    finish_out(1)
     finish_rows(3)
     x_send(3)
+
+    weight_rows(half - 1)
+    wc_copy = remote(wbuf.at[other], wc_r, "wcs", (0,), st_id=partner)
+    go(wc_copy)
     x_forward(2)
-
-    wbuf, wc_r, w1, wy_r, w2, wz_r = get("wbuf", "wc_r", "w1", "wy_r", "w2", "wz_r")
-    part = weight_ref.shape[0]
-
-    @pl.loop(0, ZN)
-    def _(k):
-        cols = pl.ds(pl.multiple_of(k * slab * part, slab * part), slab * part)
-        tile = low_dot(rows_v[:, cols], key_grad[...], CONTRACT_FIRST).astype(BF16)
-        for o in range(slab):
-            wbuf[o % CN, o // CN, k] = tile[o * part : (o + 1) * part]
-
-    wc_copy = remote(wbuf.at[other], wc_r, "wcs", (), st_id=partner)
-    go(wc_copy)
     for d in range(2):
         for copy in t_copies(1, d):
             copy.wait_recv()
         for copy in t_copies(2, d):
             go(copy)
-    for d in range(1, XN):
-        w_across(d).wait_recv()
-        gw_copy(d).wait_recv()
-    finish_out(0)
     wc_copy.wait_recv()
     for yi in range(YN):
         w1[yi] = (wbuf[c, yi].astype(F32) + wc_r[yi].astype(F32)).astype(BF16)
 
     def wy_copy(d):
-        return remote(w1.at[ys[d]], wy_r.at[d], "wys", (d,), st_id=at(z, ys[d], c))
+        return remote(w1.at[ys[d]], wy_r.at[d], "wys", (0,), st_id=at(z, ys[d], c))
 
     def wz_copy(d):
-        return remote(w2.at[zs[d]], wz_r.at[d], "wzs", (d,), st_id=at(zs[d], y, c))
+        return remote(w2.at[zs[d]], wz_r.at[d], "wzs", (0,), st_id=at(zs[d], y, c))
 
     for d in (2, 1, 3):
         go(wy_copy(d))
-    finish_out(1)
+    finish_out(2)
     x_forward(3)
-    for d in range(1, YN):
-        wy_copy(d).wait_recv()
+    all_of(wy_r.at[pl.ds(1, YN - 1)], "wys", (0,)).wait_recv()
     gathered = w1[y].astype(F32)
     for d in range(1, YN):
         gathered += wy_r[d].astype(F32)
     w2[...] = gathered.astype(BF16)
     for d in (4, 3, 5, 2, 6, 1, 7):
         go(wz_copy(d))
-    finish_out(2)
     for d in range(2):
         for copy in t_copies(2, d):
             copy.wait_recv()
@@ -835,21 +860,45 @@
         for i in range(XN):
             value += low_dot(qga[i, here, :], weight_of(i, 2), CONTRACT_LAST)
         tok_out[here, :] = value.astype(tok_out.dtype)
-    for d in range(1, ZN):
-        wz_copy(d).wait_recv()
+        leave(1, tok_out.at[here, :], r["tok_out"].at[here, :])
+    all_of(wz_r.at[pl.ds(1, ZN - 1)], "wzs", (0,)).wait_recv()
     weight = w2[z].astype(F32)
     for d in range(1, ZN):
         weight += wz_r[d].astype(F32)
     weight_ref[...] = weight
+    leave(2, weight_ref, r["weight_ref"])
     finish_out(3)
-    for copy in started:
-        copy.wait_send()
-
-    @pl.loop(0, ZN)
-    def _(reader):
-        term_copy(reader).wait_send()
-        for d in range(1, ZN):
-            zt_copy(d, reader).wait_send()
+    moved = dict(
+        id0=(id_refs[0], "idsem"),
+        id1=(id_refs[1], "idsem"),
+        tokx=(tok4.at[pl.ds(0, XN - 1)], "tokx"),
+        cotz=(qg.at[pl.ds(0, ZN - 1)], "cotz"),
+        qz=(qg.at[pl.ds(0, ZN - 1)], "qz"),
+        gz=(gates.at[pl.ds(0, ZN - 1)], "gz"),
+        kvy=(kv.at[pl.ds(0, 3 * passes)], "kvy"),
+        kvd=(kv.at[pl.ds(0, YN * passes)], "kvd"),
+        zts=(zt_r.at[pl.ds(1, ZN - 1)], "zts"),
+        ters=(term_r, "ters"),
+        zrs=(qg.at[pl.ds(0, ZN - 1)], "zrs"),
+        yfs=(yf_s, "yfs"),
+        yds=(yd_s, "yds"),
+        xrs=(kgv.at[pl.ds(0, 3)], "xrs"),
+        tgs=(qga.at[pl.ds(0, 3)], "tgs"),
+        ggs=(gga.at[pl.ds(0, 3)], "ggs"),
+        wxs=(w_all.at[pl.ds(0, XN - 1), 0], "wxs"),
+        wxd=(w_all.at[pl.ds(0, XN - 1), 0], "wxd"),
+        gws=(gw_all.at[pl.ds(0, XN - 1)], "gws"),
+        wcs=(wc_r, "wcs"),
+        wys=(wy_r.at[pl.ds(1, YN - 1)], "wys"),
+        wzs=(wz_r.at[pl.ds(1, ZN - 1)], "wzs"),
+    )
+    for group, (ref, sem) in moved.items():
+        index = (0,) * len(r[sem].shape)
+        all_of(ref, sem, index, group).wait_send()
+    for index, (src, dst) in enumerate(
+        ((out_ref, "out_ref"), (tok_out, "tok_out"), (weight_ref, "weight_ref"))
+    ):
+        pltpu.make_async_copy(src, r[dst], r["outs"].at[index]).wait()
 
 
 def fused_call(rate, ids, gate_w, beta, decay, tok, cot, mq, mk, mv, qw, kw, vw, rows):
@@ -870,7 +919,7 @@
             jax.ShapeDtypeStruct((part, head), F32),
         ),
         in_specs=[SMEM_SPEC] + [VMEM_SPEC] * 4 + [ANY_SPEC] * 9,
-        out_specs=(VMEM_SPEC,) * 3,
+        out_specs=(ANY_SPEC,) * 3,
         scratch_shapes=[pltpu.VMEM(*v) for v in vmem.values()]
         + [pltpu.SMEM((2, CN * ZN, 128), jnp.int32)]
         + [DMA(s) for s in sems.values()],

time: 137 us -> 133 us (0.971)
  Pallas kernels: 133 us -> 129 us
    pallas_call x1, Pallas kernels: 131 us -> 127 us  [fused_call(): pl.pallas_call(functools.partial(fused_kernel, names), out_shape=(jax.Sha...]
where the time goes in v4:
time: 133 us; the launch traced here: 131 us
  Pallas kernels  129 us (97%)
  local copies, waits for them, and re-layouts  1.45 us (1%)
    pallas_call x1, Pallas kernels, fused_call(): pl.pallas_call(functools.partial(fused_kernel, names), out_shape=(jax.Sha...  127 us

profile of v4, /device:TPU:1, one launch (start us, length us, event | category | flops | bytes accessed | tf_op | source)
XLA Modules:
  0.0 131.2 jit_solution(7910484496994983752)
XLA Ops:
  0.6 0.8 copy.18
  1.4 0.1 reshape.15
  1.5 0.6 pad.4.refs_1_
  2.1 126.6 %fused.1 = (bf16[384,512]{1,0:T(8,128)(2,1)}, bf16[1024,512]{1,0:T(8,128)(2,1)}, f32[32,256]{1,0:T(8,128)}) custom-call(f32[2]{0:T(128)} %refs_0_.1, s32[8,128]{1,0:T(8,128)} %pad.4.refs_1_, bf16[1,2048]{1,0:T(2,128)(2,1)} %refs_2_.1, f32[2,384]{1,0:T(2,128)} %refs_3_.1, f32[2,384]{1,0:T(2,128)} %refs_4_.1, bf16[384,512]{1,0:T(8,128)(2,1)} %refs_5_.1, ...), custom_call_target="tpu_custom_call" | custom-call | tf_op jit(solution)/shard_map/fused/pallas_call | solution.py:914
  128.7 2.5 %settle.1 = (bf16[384,512]{1,0:T(8,128)(2,1)}, bf16[1024,512]{1,0:T(8,128)(2,1)}, f32[32,256]{1,0:T(8,128)}) custom-call(bf16[384,512]{1,0:T(8,128)(2,1)} %get-tuple-element.9.refs_0_, bf16[1024,512]{1,0:T(8,128)(2,1)} %get-tuple-element.10.refs_1_, f32[32,256]{1,0:T(8,128)} %get-tuple-element.11.refs_2_), custom_call_target="tpu_custom_call" | custom-call | tf_op jit(solution)/shard_map/settle/pallas_call | solution.py:38

commit v5 on v4

--- a/solution.py
+++ b/solution.py
@@ -29,17 +29,37 @@
 
 
 def settle_kernel(*refs):
-    count = len(refs) // 2
-    for source, target in zip(refs[:count], refs[count:]):
-        target[...] = source[...]
+    count = (len(refs) - 1) // 3
+    sources, targets, buffers, sems = refs[:count], refs[count : 2 * count], refs[2 * count : -1], refs[-1]
+    moves = []
+    for source, target, buffer in zip(sources, targets, buffers):
+        pieces = 4 if source.shape[0] >= 512 else 1
+        rows = source.shape[0] // pieces
+        for k in range(pieces):
+            here = pl.ds(k * rows, rows)
+            n = len(moves)
+            moves.append(
+                (
+                    pltpu.make_async_copy(source.at[here, :], buffer.at[here, :], sems.at[0, n]),
+                    pltpu.make_async_copy(buffer.at[here, :], target.at[here, :], sems.at[1, n]),
+                )
+            )
+    for inward, _ in moves:
+        inward.start()
+    for inward, outward in moves:
+        inward.wait()
+        outward.start()
+    for _, outward in moves:
+        outward.wait()
 
 
 def settle_call(*arrays):
     return pl.pallas_call(
         settle_kernel,
         out_shape=tuple(jax.ShapeDtypeStruct(x.shape, x.dtype) for x in arrays),
-        in_specs=[VMEM_SPEC] * len(arrays),
-        out_specs=(VMEM_SPEC,) * len(arrays),
+        in_specs=[ANY_SPEC] * len(arrays),
+        out_specs=(ANY_SPEC,) * len(arrays),
+        scratch_shapes=[pltpu.VMEM(x.shape, x.dtype) for x in arrays] + [DMA((2, 6))],
         name="settle",
     )(*arrays)
 
@@ -109,6 +129,7 @@
         mv=((tok_n, head), BF16),
         ids_all=((CN, ZN, 8, 128), jnp.int32),
         tab_v=((2, CN * ZN, 128), jnp.int32),
+        ids_v=((8, 128), jnp.int32),
         code=((YN, CN, 8, ZN * BLOCK), jnp.int32),
         turned=((tok_n, 8), F32),
         mixed=((tok_n, head), F32),
@@ -273,6 +294,14 @@
     load("mv", r["mv_h"], r["mv"])
     load("qw", r["qw_h"], qw)
 
+    id_lane = lax.broadcasted_iota(jnp.int32, (8, 128), 1)
+    id_row = jnp.zeros((8, 128), jnp.int32)
+    per_block, blocks_n = ids.shape
+    for b in range(blocks_n):
+        for k in range(per_block):
+            id_row = jnp.where(id_lane == b * per_block + k, ids[k, b], id_row)
+    r["ids_v"][...] = id_row
+
     barrier = pltpu.get_barrier_semaphore()
     greeted = 0
     for target in xs[1:]:
@@ -314,7 +343,7 @@
 
     def ids_copy(dc, dz):
         return remote(
-            ids,
+            r["ids_v"],
             r["ids_all"].at[c, z],
             "idsem",
             (dc,),
@@ -325,7 +354,7 @@
     id_peers = [(dc, dz) for dz in range(ZN) for dc in range(CN) if (dc, dz) != (0, 0)]
     for dc, dz in id_peers:
         go(ids_copy(dc, dz))
-    r["ids_all"][c, z] = ids[...]
+    r["ids_all"][c, z] = id_row
     loads["tok"].wait()
     for d in range(2):
         go(tok_copy(1, d, d))
@@ -508,7 +537,6 @@
     q_pass(3, True)
     q_pass(3, False)
     q_pass(4, True)
-    pl.loop(4, 5)(mix)
     tab_copy.wait()
     lane_of = lax.broadcasted_iota(jnp.int32, (8, ZN * BLOCK), 1)
     for yi in range(YN):
@@ -752,10 +780,11 @@
     all_of(term_r, "ters", (0,)).wait_recv()
 
     y_send(0)
-    pl.loop(5, spans_n)(mix)
+    pl.loop(4, 5)(mix)
     y_forward(0)
     y_send(1)
     z_pass(2)
+    pl.loop(5, spans_n)(mix)
     finish_rows(0)
     x_send(0)
     y_forward(1)
@@ -823,24 +852,23 @@
     wc_copy = remote(wbuf.at[other], wc_r, "wcs", (0,), st_id=partner)
     go(wc_copy)
     x_forward(2)
+    wc_copy.wait_recv()
+    for yi in range(YN):
+        w1[yi] = (wbuf[c, yi].astype(F32) + wc_r[yi].astype(F32)).astype(BF16)
+
+    def wy_copy(d):
+        return remote(w1.at[ys[d]], wy_r.at[d], "wys", (0,), st_id=at(z, ys[d], c))
+
+    def wz_copy(d):
+        return remote(w2.at[zs[d]], wz_r.at[d], "wzs", (0,), st_id=at(zs[d], y, c))
+
+    for d in (2, 1, 3):
+        go(wy_copy(d))
     for d in range(2):
         for copy in t_copies(1, d):
             copy.wait_recv()
         for copy in t_copies(2, d):
             go(copy)
-    wc_copy.wait_recv()
-    for yi in range(YN):
-        w1[yi] = (wbuf[c, yi].astype(F32) + wc_r[yi].astype(F32)).astype(BF16)
-
-    def wy_copy(d):
-        return remote(w1.at[ys[d]], wy_r.at[d], "wys", (0,), st_id=at(z, ys[d], c))
-
-    def wz_copy(d):
-        return remote(w2.at[zs[d]], wz_r.at[d], "wzs", (0,), st_id=at(zs[d], y, c))
-
-    for d in (2, 1, 3):
-        go(wy_copy(d))
-    finish_out(2)
     x_forward(3)
     all_of(wy_r.at[pl.ds(1, YN - 1)], "wys", (0,)).wait_recv()
     gathered = w1[y].astype(F32)
@@ -849,6 +877,7 @@
     w2[...] = gathered.astype(BF16)
     for d in (4, 3, 5, 2, 6, 1, 7):
         go(wz_copy(d))
+    finish_out(2)
     for d in range(2):
         for copy in t_copies(2, d):
             copy.wait_recv()
@@ -918,7 +947,7 @@
             jax.ShapeDtypeStruct((rows_n, width), BF16),
             jax.ShapeDtypeStruct((part, head), F32),
         ),
-        in_specs=[SMEM_SPEC] + [VMEM_SPEC] * 4 + [ANY_SPEC] * 9,
+        in_specs=[SMEM_SPEC] * 2 + [VMEM_SPEC] * 3 + [ANY_SPEC] * 9,
         out_specs=(ANY_SPEC,) * 3,
         scratch_shapes=[pltpu.VMEM(*v) for v in vmem.values()]
         + [pltpu.SMEM((2, CN * ZN, 128), jnp.int32)]
@@ -948,11 +977,9 @@
 ):
     pass_local, span_rows, model_width = passages.shape
     flat_rows = passages.reshape(pass_local * span_rows, model_width)
-    req_count = passage_ids.size
-    ids = jnp.pad(passage_ids.reshape(1, req_count), ((0, 7), (0, -req_count % 128)))
     token_grad, passage_grad, key_weight_grad = fused_call(
         decay_rate,
-        ids,
+        passage_ids.T,
         gate_weight,
         beta_pre,
         decay_pre,

time: 133 us -> 130 us (0.977)
  local copies, waits for them, and re-layouts: 1.45 us -> 0 us
where the time goes in v5:
time: 130 us; the launch traced here: 129 us
  Pallas kernels  128 us (98%)
    pallas_call x1, Pallas kernels, fused_call(): pl.pallas_call(functools.partial(fused_kernel, names), out_shape=(jax.Sha...  126 us

profile of v5, /device:TPU:1, one launch (start us, length us, event | category | flops | bytes accessed | tf_op | source)
XLA Modules:
  0.0 128.8 jit_solution(8342253937816209648)
XLA Ops:
  0.6 125.7 %fused.1 = (bf16[384,512]{1,0:T(8,128)(2,1)}, bf16[1024,512]{1,0:T(8,128)(2,1)}, f32[32,256]{1,0:T(8,128)}) custom-call(f32[2]{0:T(128)} %refs_0_.1, s32[4,6]{1,0:T(4,128)} %bitcast.4, bf16[1,2048]{1,0:T(2,128)(2,1)} %refs_2_.1, f32[2,384]{1,0:T(2,128)} %refs_3_.1, f32[2,384]{1,0:T(2,128)} %refs_4_.1, bf16[384,512]{1,0:T(8,128)(2,1)} %refs_5_.1, ...), custom_call_target="tpu_custom_call" | custom-call | tf_op jit(solution)/shard_map/fused/pallas_call | solution.py:943
  126.4 2.2 %settle.1 = (bf16[384,512]{1,0:T(8,128)(2,1)}, bf16[1024,512]{1,0:T(8,128)(2,1)}, f32[32,256]{1,0:T(8,128)}) custom-call(bf16[384,512]{1,0:T(8,128)(2,1)} %get-tuple-element.9.refs_0_, bf16[1024,512]{1,0:T(8,128)(2,1)} %get-tuple-element.10.refs_1_, f32[32,256]{1,0:T(8,128)} %get-tuple-element.11.refs_2_), custom_call_target="tpu_custom_call" | custom-call | tf_op jit(solution)/shard_map/settle/pallas_call | solution.py:57

commit v6 on v5

--- a/solution.py
+++ b/solution.py
@@ -146,13 +146,12 @@
         terms=((CN, ZN, YN, BLOCK, 2 * head), BF16),
         term_r=((ZN, YN, BLOCK, 2 * head), BF16),
         qg=((ZN, tok_n, head), BF16),
-        z_s=((2, ZN // 2, tok_n, head), BF16),
+        z_s=((2, ZN // 2 - 1, tok_n, head), BF16),
         z_r=((2, ZN // 2, tok_n, head), BF16),
         yf_s=((2, half, ROW, 2 * head), BF16),
         yf_r=((2, half, ROW, 2 * head), BF16),
         yd_s=((2, chunks, ROW, 2 * head), BF16),
         yd_r=((2, chunks, ROW, 2 * head), BF16),
-        key_grad=((rows_n, head), BF16),
         kgv=((XN, rows_n, 2 * head), BF16),
         qga=((XN, tok_n, head), BF16),
         gga=((XN, 8, tok_n), F32),
@@ -169,6 +168,8 @@
         out_v=((rows_n, width), BF16),
         weight_v=((part, head), F32),
         w_acc=((model, head), F32),
+        out_part=((2, 2, ROW, width), F32),
+        tok_part=((tok_n, width), F32),
     )
     sems = dict(
         load=(16,),
@@ -186,7 +187,7 @@
         zrs=(2, ZN // 2),
         yfs=(2, half),
         yds=(chunks,),
-        xrs=(2, chunks),
+        xrs=(3, chunks),
         tgs=(2, 2),
         ggs=(2, 2),
         wxs=(1,),
@@ -213,7 +214,7 @@
     tab_v, tab_s, code = get("tab_v", "tab_s", "code")
     kvr, e_buf, g_buf, sg, pg, zt, zt_r = get("kvr", "e_buf", "g_buf", "sg", "pg", "zt", "zt_r")
     terms, term_r, qg, z_s, z_r = get("terms", "term_r", "qg", "z_s", "z_r")
-    key_low, key_grad, query_low = get("key_low", "key_grad", "query_low")
+    key_low, query_low = get("key_low", "query_low")
     kgv, qga, gga, w_all, gwb, gw_all = get("kgv", "qga", "gga", "w_all", "gwb", "gw_all")
     turned, mixed, states = get("turned", "mixed", "states")
 
@@ -551,13 +552,13 @@
                 )
                 start = jnp.where(lax.shift_right_logical(lane_of, 6) == zi, base, start)
             code[yi, which] = start + (lane_of & (BLOCK - 1))
+    for d, k in ((0, 0), (1, 2), (0, 1), (1, 3)):
+        kv_copy(2, d, k).wait_recv()
+        go(kv_across(2, k))
     for d in range(2):
         cot_copy(ZN // 2, d).wait_recv()
         for copy in q_copies(ZN // 2 - 1, d, 1 - d) + q_copies(ZN // 2, d, d):
             copy.wait_recv()
-    for d, k in ((0, 0), (1, 2), (0, 1), (1, 3)):
-        kv_copy(2, d, k).wait_recv()
-        go(kv_across(2, k))
     kv_across_all = all_of(kv.at[pl.ds(0, YN * passes)], "kvd", (0,))
     kv_across_all.wait_recv()
 
@@ -636,7 +637,7 @@
             src = qg.at[zs[ZN // 2], half_rows[d]]
             dst = z_r.at[d, 0, half_rows[d]]
         else:
-            src = z_s.at[d, hop - 1]
+            src = z_s.at[d, hop - 2]
             dst = z_r.at[d, hop - 1]
         return remote(src, dst, "zrs", (d, hop - 1), st_id=z_to[d])
 
@@ -647,12 +648,12 @@
             target = zs[away] if d == 0 else zs[(-away) % ZN]
             if hop == 2:
                 mid, rest = half_rows[d], half_rows[1 - d]
-                z_s[d, hop - 1, mid, :] = (
+                z_s[d, hop - 2, mid, :] = (
                     qg[target, mid, :].astype(F32) + z_r[d, 0, mid, :].astype(F32)
                 ).astype(BF16)
-                z_s[d, hop - 1, rest, :] = qg[target, rest, :]
+                z_s[d, hop - 2, rest, :] = qg[target, rest, :]
             else:
-                z_s[d, hop - 1] = (
+                z_s[d, hop - 2] = (
                     qg[target].astype(F32) + z_r[d, hop - 2].astype(F32)
                 ).astype(BF16)
             go(z_copy(hop, d))
@@ -711,8 +712,8 @@
     def x_copy(hop, d, q):
         source = x if hop == 1 else (xs[XN - 1] if d == 0 else xs[1])
         ref = kgv.at[source, pl.ds(q * ROW, ROW)]
-        passed_on = hop == 1 and (q < half) == (d == 0)
-        return remote(ref, ref, "xrs", (0 if passed_on else 1, q), tp_id=x_to[d])
+        kind = 2 if hop == 2 else 0 if (q < half) == (d == 0) else 1
+        return remote(ref, ref, "xrs", (kind, q), tp_id=x_to[d])
 
     def x_send(j):
         for q in (j, j + half):
@@ -739,20 +740,42 @@
                 scale * hat
                 - scale * scale * scale * low * jnp.mean(low * hat, axis=-1, keepdims=True)
             ).astype(BF16)
-            key_grad[here, :] = grad
             kgv[x, here, :head] = grad
             kgv[x, here, head:] = value[:, head:].astype(BF16)
+
+    def rows_of(q, rels):
+        here = pl.ds(q * ROW, ROW)
+        value = jnp.zeros((ROW, width), F32)
+        for rel in rels:
+            i = xs[rel]
+            value += low_dot(kgv[i, here, :head], weight_of(i, 0), CONTRACT_LAST)
+            value += low_dot(kgv[i, here, head:], weight_of(i, 1), CONTRACT_LAST)
+        return value
+
+    near_heads, far_head = (0, 1, 3), (2,)
+    out_part, tok_part = get("out_part", "tok_part")
+
+    def near_out(j):
+        for d in range(2):
+            q = j + half * d
+            x_copy(1, 1 - d, q).wait_recv()
+            out_part[j - half + 2, d] = rows_of(q, near_heads)
+
+    def far_out(j):
+        for d in range(2):
+            q = j + half * d
+            here = pl.ds(q * ROW, ROW)
+            x_copy(2, d, q).wait_recv()
+            out_ref[here, :] = (out_part[j - half + 2, d] + rows_of(q, far_head)).astype(out_ref.dtype)
+            leave(0, out_ref.at[here, :], r["out_ref"].at[here, :])
 
     def finish_out(j):
         for d in range(2):
             q = j + half * d
             here = pl.ds(q * ROW, ROW)
-            all_of(kgv.at[pl.ds(0, 2), here], "xrs", (1, q)).wait_recv()
-            value = jnp.zeros((ROW, width), F32)
-            for i in range(XN):
-                value += low_dot(kgv[i, here, :head], weight_of(i, 0), CONTRACT_LAST)
-                value += low_dot(kgv[i, here, head:], weight_of(i, 1), CONTRACT_LAST)
-            out_ref[here, :] = value.astype(out_ref.dtype)
+            x_copy(1, 1 - d, q).wait_recv()
+            x_copy(2, d, q).wait_recv()
+            out_ref[here, :] = rows_of(q, range(XN)).astype(out_ref.dtype)
             leave(0, out_ref.at[here, :], r["out_ref"].at[here, :])
 
     wbuf, wc_r, w1, wy_r, w2, wz_r = get("wbuf", "wc_r", "w1", "wy_r", "w2", "wz_r")
@@ -761,7 +784,7 @@
 
     def weight_rows(j):
         low, high = pl.ds(j * ROW, ROW), pl.ds((j + half) * ROW, ROW)
-        grad = jnp.concatenate([key_grad[low, :], key_grad[high, :]], axis=0)
+        grad = jnp.concatenate([kgv[x, low, :head], kgv[x, high, :head]], axis=0)
 
         @pl.loop(0, ZN)
         def _(k):
@@ -869,6 +892,13 @@
             copy.wait_recv()
         for copy in t_copies(2, d):
             go(copy)
+    for k in range(tok_n // ROW):
+        here = pl.ds(k * ROW, ROW)
+        value = jnp.zeros((ROW, width), F32)
+        for rel in near_heads:
+            value += low_dot(qga[xs[rel], here, :], weight_of(xs[rel], 2), CONTRACT_LAST)
+        tok_part[here, :] = value
+    near_out(2)
     x_forward(3)
     all_of(wy_r.at[pl.ds(1, YN - 1)], "wys", (0,)).wait_recv()
     gathered = w1[y].astype(F32)
@@ -877,7 +907,8 @@
     w2[...] = gathered.astype(BF16)
     for d in (4, 3, 5, 2, 6, 1, 7):
         go(wz_copy(d))
-    finish_out(2)
+    near_out(3)
+    far_out(2)
     for d in range(2):
         for copy in t_copies(2, d):
             copy.wait_recv()
@@ -886,8 +917,9 @@
     for k in range(tok_n // ROW):
         here = pl.ds(k * ROW, ROW)
         value = exact_dot(gate_rows[:, k * ROW : (k + 1) * ROW], gate_cols, CONTRACT_FIRST)
-        for i in range(XN):
-            value += low_dot(qga[i, here, :], weight_of(i, 2), CONTRACT_LAST)
+        value += tok_part[here, :] + low_dot(
+            qga[xs[2], here, :], weight_of(xs[2], 2), CONTRACT_LAST
+        )
         tok_out[here, :] = value.astype(tok_out.dtype)
         leave(1, tok_out.at[here, :], r["tok_out"].at[here, :])
     all_of(wz_r.at[pl.ds(1, ZN - 1)], "wzs", (0,)).wait_recv()
@@ -896,7 +928,7 @@
         weight += wz_r[d].astype(F32)
     weight_ref[...] = weight
     leave(2, weight_ref, r["weight_ref"])
-    finish_out(3)
+    far_out(3)
     moved = dict(
         id0=(id_refs[0], "idsem"),
         id1=(id_refs[1], "idsem"),

time: 130 us -> 130 us (level); the launches traced: 129 us -> 130 us
    pallas_call x1, Pallas kernels: 126 us -> 127 us  [fused_call(): pl.pallas_call(functools.partial(fused_kernel, names), out_shape=(jax.Sha...]
where the time goes in v6:
time: 130 us
  Pallas kernels  129 us (99%)
    pallas_call x1, Pallas kernels, fused_call(): pl.pallas_call(functools.partial(fused_kernel, names), out_shape=(jax.Sha...  127 us

profile of v6, /device:TPU:1, one launch (start us, length us, event | category | flops | bytes accessed | tf_op | source)
XLA Modules:
  0.0 130.1 jit_solution(16237866963028093399)
XLA Ops:
  0.6 127.1 %fused.1 = (bf16[384,512]{1,0:T(8,128)(2,1)}, bf16[1024,512]{1,0:T(8,128)(2,1)}, f32[32,256]{1,0:T(8,128)}) custom-call(f32[2]{0:T(128)} %refs_0_.1, s32[4,6]{1,0:T(4,128)} %bitcast.4, bf16[1,2048]{1,0:T(2,128)(2,1)} %refs_2_.1, f32[2,384]{1,0:T(2,128)} %refs_3_.1, f32[2,384]{1,0:T(2,128)} %refs_4_.1, bf16[384,512]{1,0:T(8,128)(2,1)} %refs_5_.1, ...), custom_call_target="tpu_custom_call" | custom-call | tf_op jit(solution)/shard_map/fused/pallas_call | solution.py:975
  127.8 2.2 %settle.1 = (bf16[384,512]{1,0:T(8,128)(2,1)}, bf16[1024,512]{1,0:T(8,128)(2,1)}, f32[32,256]{1,0:T(8,128)}) custom-call(bf16[384,512]{1,0:T(8,128)(2,1)} %get-tuple-element.9.refs_0_, bf16[1024,512]{1,0:T(8,128)(2,1)} %get-tuple-element.10.refs_1_, f32[32,256]{1,0:T(8,128)} %get-tuple-element.11.refs_2_), custom_call_target="tpu_custom_call" | custom-call | tf_op jit(solution)/shard_map/settle/pallas_call | solution.py:57
